TPU v7x, 32 devices: a whole 2x2x4 slice. The times are simulated.
32 devices in a mesh: sp: 8 (over z, x), tp: 4 (over y, core).
Axes of the slice: x: 2, y: 2, z: 4, core: 2. Of those that a mesh axis runs over, the one named last changes fastest.
Arguments:
- tokens: bfloat16 [4096, 2048], P(('sp', 'tp')), may hold values from -6 to 6
- norm_gain: float32 [2048], replicated, may hold values from 0.1 to 1.9
- rec_query: bfloat16 [2048, 1024], P(None, 'tp'), may hold values from -0.125 to 0.125
- fwd_gate: bfloat16 [2048, 1024], P(None, 'tp'), may hold values from -0.125 to 0.125
- bwd_gate: bfloat16 [2048, 1024], P(None, 'tp'), may hold values from -0.125 to 0.125
- rec_value: bfloat16 [2048, 1024], P(None, 'tp'), may hold values from -0.125 to 0.125
- gate_leak: float32 [2, 1024], P(None, 'tp'), may hold values from 0 to 0.08, as said below
- log_decay: float32 [2, 4096, 8], P(None, 'sp', 'tp'), may hold values from -2.2 to 0, as said below
- rec_gain: float32 [128], replicated, may hold values from 0.1 to 1.9
- att_query: bfloat16 [2048, 1024], P(None, 'tp'), as said below
- att_key: bfloat16 [2048, 1024], P(None, 'tp')
- att_value: bfloat16 [2048, 1024], P(None, 'tp'), may hold values from -0.125 to 0.125
- lambdas: float32 [8], P('tp'), may hold values from 0.3 to 0.8
- att_gain: float32 [128], replicated, may hold values from 0.1 to 1.9
- out_rec: bfloat16 [1024, 2048], replicated, may hold values from -0.125 to 0.125
- out_att: bfloat16 [1024, 2048], replicated, may hold values from -0.125 to 0.125
Outputs:
- layer_out: bfloat16 [4096, 2048], P(('sp', 'tp'))
Inputs may be any that keep to these rules, and one draw needn't show every extreme that they name: `gate_leak`: positive, by direction and channel. `log_decay`: never positive. `att_query`: entries of order 2048 to the power -1/2.
All inputs are finite; a program needn't handle non-finite values.
Results may differ from a plain program's by a relative error of at most 0.011.
Values may be sent and summed in bfloat16 or wider, within the bound.
A program may use at most 128 MiB of HBM per device.

v0:
```python
import functools

import jax
import jax.numpy as jnp
from jax import lax
from jax.experimental import pallas as pl
from jax.experimental.pallas import tpu as pltpu
from jax.sharding import PartitionSpec as P

HK = 128
AK = 64
BLOCK = 64
LANES = 128
EPS = 1e-06
THETA = 500000.0
HIGHEST = lax.Precision.HIGHEST
F32 = jnp.float32
BF16 = jnp.bfloat16
PAD = 16


def rms_scale(values, gain):
    return values * lax.rsqrt(jnp.mean(values * values, axis=-1, keepdims=True) + EPS) * gain


def dot_t(a, b):
    return lax.dot_general(a, b, (((1,), (1,)), ((), ())), preferred_element_type=F32)


def dot_0(a, b):
    return lax.dot_general(a, b, (((0,), (0,)), ((), ())), preferred_element_type=F32)


def gather_kernel(tp, tokens, gain, *refs):
    weights, outs = refs[:7], refs[7:14]
    held, across, along, landed = refs[14:]
    me = lax.axis_index("tp")
    core = lax.rem(me, 2)
    pair = lax.div(me, 2)
    pairs = tp // 2
    count = tokens.shape[0]
    partner = pair * 2 + 1 - core
    others = [lax.rem(pair + k, pairs) for k in range(1, pairs)]
    barrier = pltpu.get_barrier_semaphore()
    pl.semaphore_signal(barrier, inc=1, device_id={"tp": partner})
    for q in others:
        pl.semaphore_signal(barrier, inc=1, device_id={"tp": q * 2 + core})

    def rows_at(block):
        return held.at[pl.ds(pl.multiple_of(block * count, count), count)]

    def to_partner(block):
        return pltpu.make_async_remote_copy(
            src_ref=rows_at(block),
            dst_ref=rows_at(block),
            send_sem=across.at[block],
            recv_sem=landed.at[block],
            device_id={"tp": partner},
        )

    def to_pair(q):
        return pltpu.make_async_remote_copy(
            src_ref=rows_at(me),
            dst_ref=rows_at(me),
            send_sem=along.at[q],
            recv_sem=landed.at[me],
            device_id={"tp": q * 2 + core},
        )

    normed = rms_scale(tokens[...].astype(F32), gain[...]).astype(BF16)
    held[pl.ds(pl.multiple_of(me * count, count), count), :] = normed
    pl.semaphore_wait(barrier, pairs)
    for q in others:
        to_pair(q).start()
    to_partner(me).start()

    def step(k, carry):
        q = lax.rem(pair + k, pairs)
        near = q * 2 + core

        @pl.when(k > 0)
        def _():
            to_partner(near).wait_recv()
            to_partner(near).start()

        to_partner(q * 2 + 1 - core).wait_recv()
        at = pl.ds(pl.multiple_of(q * 2 * count, 2 * count), 2 * count)
        for weight, result in zip(weights, outs):
            result[at, :] = jnp.dot(held[at, :], weight[...], preferred_element_type=F32).astype(BF16)
        return carry

    lax.fori_loop(0, pairs, step, 0)
    to_partner(me).wait_send()
    for q in others:
        to_pair(q).wait_send()
        to_partner(q * 2 + core).wait_send()


def mixer_kernel(
    ranks, tp, groups, heads, tile,
    proj_k, proj_v, proj_q, proj_rq, proj_fwd, proj_bwd, proj_rv, cosine, sine, leak, decay, lam, rec_gain, att_gain,
    out,
    kv, rest, swap, stage, state_out, state_in, cums, adds, states, rec_sum, peak, total, mixed,
    kv_send, kv_recv, swap_send, rest_recv, state_send, state_recv, out_send, out_recv,
):
    me = lax.axis_index("sp")
    slot = lax.rem(me, groups)
    mine = lax.div(me, groups)
    mesh_column = lax.axis_index("tp")
    length = proj_k.shape[0]
    piece = length // tp
    rows = groups * length
    width = heads * LANES
    block_count = rows // BLOCK
    partner_slot = groups - 1 - slot
    partner = mine * groups + partner_slot
    blocks = ranks // groups
    own_rows = pl.ds(pl.multiple_of(slot * length, length), length)
    other_rows = pl.ds(pl.multiple_of(partner_slot * length, length), length)

    barrier = pltpu.get_barrier_semaphore()
    peers = []
    for k in range(1, blocks):
        peers.append(lax.rem(mine + k, blocks))
    for peer in peers:
        pl.semaphore_signal(barrier, inc=1, device_id={"sp": peer * groups + slot})
    owners = []
    for dp in range(groups):
        for dt in range(tp):
            owners.append((dp, dt, lax.rem(slot + dp, groups), lax.rem(mesh_column + dt, tp)))
    for dp, dt, p, t in owners[1:]:
        pl.semaphore_signal(barrier, inc=1, device_id={"sp": mine * groups + p, "tp": t})

    lane = lax.broadcasted_iota(jnp.int32, (length, LANES), 1)
    low_half = lax.rem(lane, AK) < AK // 2

    def rotated(raw):
        wide = raw.astype(F32)
        turned = jnp.where(low_half, -pltpu.roll(wide, LANES - AK // 2, 1), pltpu.roll(wide, AK // 2, 1))
        return wide * cosine[...] + turned * sine[...]

    def prepare(head_group, key_value, others):
        def taken(ref, h):
            return ref[:, pl.ds(pl.multiple_of((head_group * heads + h) * LANES, LANES), LANES)]

        for h in range(heads):
            at = h * LANES
            key_value[:, at : at + LANES] = rotated(taken(proj_k, h)).astype(BF16)
            key_value[:, width + at : width + at + LANES] = taken(proj_v, h)
            others[:, at : at + LANES] = (rotated(taken(proj_q, h)) * AK ** (-0.5)).astype(BF16)
            for i, ref in enumerate((proj_rq, proj_fwd, proj_bwd, proj_rv)):
                others[:, (i + 1) * width + at : (i + 1) * width + at + LANES] = taken(ref, h)

    if groups > 1:
        prepare(partner_slot, swap.at[:, : 2 * width], swap.at[:, 2 * width :])
    prepare(slot, kv.at[mine, own_rows], rest.at[own_rows])
    pl.semaphore_wait(barrier, blocks - 1 + groups * tp - 1)

    def block_copy(source_rows, source_slot, peer):
        return pltpu.make_async_remote_copy(
            src_ref=kv.at[mine, source_rows],
            dst_ref=kv.at[mine, source_rows],
            send_sem=kv_send.at[peer, source_slot],
            recv_sem=kv_recv.at[mine, source_slot],
            device_id={"sp": peer * groups + slot},
        )

    def arrival(block, piece):
        piece_rows = pl.ds(pl.multiple_of(piece * length, length), length)
        return pltpu.make_async_remote_copy(
            src_ref=kv.at[block, piece_rows],
            dst_ref=kv.at[block, piece_rows],
            send_sem=kv_send.at[block, piece],
            recv_sem=kv_recv.at[block, piece],
            device_id={"sp": block * groups + slot},
        )

    if groups > 1:
        swap_kv = pltpu.make_async_remote_copy(
            src_ref=swap.at[:, : 2 * width],
            dst_ref=kv.at[mine, own_rows],
            send_sem=swap_send.at[0],
            recv_sem=kv_recv.at[mine, slot],
            device_id={"sp": partner},
        )
        swap_kv.start()
        swap_rest = pltpu.make_async_remote_copy(
            src_ref=swap.at[:, 2 * width :],
            dst_ref=rest.at[own_rows],
            send_sem=swap_send.at[1],
            recv_sem=rest_recv,
            device_id={"sp": partner},
        )
    own_copies = [block_copy(own_rows, slot, peer) for peer in peers]
    for copy in own_copies:
        copy.start()
    other_copies = []
    if groups > 1:
        swap_rest.start()
        arrival(mine, partner_slot).wait_recv()
        other_copies = [block_copy(other_rows, partner_slot, peer) for peer in peers]
        for copy in other_copies:
            copy.start()
        swap_rest.wait_recv()

    row_at = lax.broadcasted_iota(jnp.int32, (BLOCK, BLOCK), 0)
    col_at = lax.broadcasted_iota(jnp.int32, (BLOCK, BLOCK), 1)
    earlier = (row_at >= col_at, row_at <= col_at)
    triangles = tuple(mask.astype(F32) for mask in earlier)
    ends = (BLOCK - 1, 0)
    middles = (BLOCK // 2 - 1, BLOCK // 2)

    def rows_of(direction, step):
        index = step if direction == 0 else block_count - 1 - step
        return index, pl.ds(pl.multiple_of(index * BLOCK, BLOCK), BLOCK)

    def part(at, index, h):
        return rest[at, (index * heads + h) * LANES : (index * heads + h + 1) * LANES].astype(F32)

    def keys_of(at, direction, h):
        return leak[h, direction : direction + 1, :] * jax.nn.sigmoid(-part(at, 2 + direction, h))

    states[...] = jnp.zeros_like(states)
    rec_sum[...] = jnp.zeros_like(rec_sum)

    def first_pass(step, totals):
        after = []
        for h in range(heads):
            for d in range(2):
                index, at = rows_of(d, step)
                keys = keys_of(at, d, h)
                column = d * heads + h
                logs = jnp.log1p(-keys) + decay[at, column : column + 1]
                cum = jnp.dot(triangles[d], logs, precision=HIGHEST, preferred_element_type=F32)
                cums[h, d, at, :] = cum
                last = cum[ends[d] : ends[d] + 1, :]
                scaled = (keys * jnp.exp(last - cum)).astype(BF16)
                added = dot_0(part(at, 4, h).astype(BF16), scaled)
                adds[h, d, index] = added
                states[h, d] = states[h, d] * jnp.exp(last) + added
                after.append(totals[h * 2 + d] + last)
        return tuple(after)

    nothing = tuple(jnp.zeros((1, LANES), F32) for _ in range(2 * heads))
    sums = lax.fori_loop(0, block_count, first_pass, nothing, unroll=2)
    for h in range(heads):
        for d in range(2):
            state_out[d, h, :LANES, :] = states[h, d].astype(BF16)
            factor = jnp.broadcast_to(jnp.exp(sums[h * 2 + d]), (PAD, LANES))
            coarse = factor.astype(BF16)
            fine = (factor - coarse.astype(F32)).astype(BF16)
            first_row = lax.broadcasted_iota(jnp.int32, (PAD, LANES), 0) == 0
            state_out[d, h, LANES:, :] = jnp.where(first_row, coarse.astype(F32), fine.astype(F32)).astype(BF16)
    state_copies = []
    for peer in peers:
        copy = pltpu.make_async_remote_copy(
            src_ref=state_out.at[jnp.where(peer > mine, 0, 1)],
            dst_ref=state_in.at[mine],
            send_sem=state_send.at[peer],
            recv_sem=state_recv.at[mine],
            device_id={"sp": peer * groups + slot},
        )
        copy.start()
        state_copies.append(copy)

    lane_q = lax.broadcasted_iota(jnp.int32, (tile, LANES), 1)
    tiles = rows // tile
    peak[...] = jnp.full_like(peak, -jnp.inf)
    total[...] = jnp.zeros_like(total)
    mixed[...] = jnp.zeros_like(mixed)

    def attend(block):
        for h in range(heads):
            at = h * LANES

            def one_tile(index, carry):
                q_rows = pl.ds(pl.multiple_of(index * tile, tile), tile)
                queries = rest[q_rows, at : at + LANES]
                zero = jnp.zeros_like(queries)
                both = jnp.concatenate(
                    [jnp.where(lane_q < AK, queries, zero), jnp.where(lane_q < AK, zero, queries)], axis=0
                )
                scores = dot_t(both, kv[block, :, at : at + LANES])
                before = peak[h, index][:, :1]
                raised = jnp.maximum(before, jnp.max(scores, axis=-1, keepdims=True))
                shrink = jnp.exp(before - raised)
                expo = jnp.exp(scores - raised)
                sums_now = total[h, index][:, :1] * shrink + jnp.sum(expo, axis=-1, keepdims=True)
                product = jnp.dot(
                    expo.astype(BF16), kv[block, :, width + at : width + at + LANES], preferred_element_type=F32
                )
                mixed[h, index] = mixed[h, index] * shrink + product
                peak[h, index] = jnp.broadcast_to(raised, (2 * tile, LANES))
                total[h, index] = jnp.broadcast_to(sums_now, (2 * tile, LANES))
                return carry

            lax.fori_loop(0, tiles, one_tile, 0)

    attend(mine)

    def state_arrival(block):
        return pltpu.make_async_remote_copy(
            src_ref=state_out.at[0],
            dst_ref=state_in.at[block],
            send_sem=state_send.at[block],
            recv_sem=state_recv.at[block],
            device_id={"sp": block * groups + slot},
        )

    states[...] = jnp.zeros_like(states)

    def compose(d):
        def body(step, carry):
            block = step if d == 0 else blocks - 1 - step
            state_arrival(block).wait_recv()
            for h in range(heads):
                rows_last = state_in[block, h, LANES:, :].astype(F32)
                factor = rows_last[0:1] + rows_last[1:2]
                states[h, d] = states[h, d] * factor + state_in[block, h, :LANES, :].astype(F32)
            return carry

        return body

    lax.fori_loop(0, mine, compose(0), 0)
    lax.fori_loop(0, blocks - 1 - mine, compose(1), 0)

    def second_pass(step, carry):
        for h in range(heads):
            for d in range(2):
                index, at = rows_of(d, step)
                queries = jax.nn.silu(part(at, 1, h))
                keys = keys_of(at, d, h)
                cum = cums[h, d, at, :]
                middle = cum[middles[d] : middles[d] + 1, :]
                last = cum[ends[d] : ends[d] + 1, :]
                scores = dot_t(
                    (queries * jnp.exp(cum - middle)).astype(BF16), (keys * jnp.exp(middle - cum)).astype(BF16)
                )
                scores = jnp.where(earlier[d], scores, 0.0)
                within = jnp.dot(scores.astype(BF16), part(at, 4, h).astype(BF16), preferred_element_type=F32)
                before = states[h, d]
                carried = dot_t_state(queries * jnp.exp(cum), before)
                span = slice(h * LANES, (h + 1) * LANES)
                rec_sum[at, span] = rec_sum[at, span] + within + carried
                states[h, d] = before * jnp.exp(last) + adds[h, d, index]
        return carry

    def dot_t_state(reads, state):
        return dot_t(reads.astype(BF16), state.astype(BF16))

    lax.fori_loop(0, block_count, second_pass, 0, unroll=2)

    for h in range(heads):
        span = slice(h * LANES, (h + 1) * LANES)
        stage[:, span] = rms_scale(rec_sum[:, span], rec_gain[...]).astype(BF16)

    def hand_over(which, owner):
        dp, dt, p, t = owner
        columns = slice(which * width, (which + 1) * width)
        source = stage.at[pl.ds(pl.multiple_of(p * length + t * piece, piece), piece), columns]
        target = out.at[mesh_column, slot, :, columns]
        if dp == 0 and dt == 0:
            return pltpu.make_async_copy(source, target, out_send.at[which, dp, dt])
        return pltpu.make_async_remote_copy(
            src_ref=source,
            dst_ref=target,
            send_sem=out_send.at[which, dp, dt],
            recv_sem=out_recv.at[which, mesh_column, slot],
            device_id={"sp": mine * groups + p, "tp": t},
        )

    def taken_over(which, owner):
        dp, dt, p, t = owner
        columns = slice(which * width, (which + 1) * width)
        target = out.at[t, p, :, columns]
        return pltpu.make_async_remote_copy(
            src_ref=target,
            dst_ref=target,
            send_sem=out_send.at[which, dp, dt],
            recv_sem=out_recv.at[which, t, p],
            device_id={"sp": mine * groups + p, "tp": t},
        )

    for owner in owners:
        hand_over(0, owner).start()

    def next_block(turn, carry):
        near = lax.div(turn + 1, 2)
        away = jnp.where(lax.rem(turn, 2) == 1, near, blocks - near)
        block = lax.rem(mine + away, blocks)
        for piece in range(groups):
            arrival(block, piece).wait_recv()
        attend(block)
        return carry

    lax.fori_loop(1, blocks, next_block, 0)

    for h in range(heads):
        span = slice(width + h * LANES, width + (h + 1) * LANES)
        for index in range(tiles):
            ratio = mixed[h, index] / total[h, index][:, :1]
            values = ratio[:tile] - lam[h] * ratio[tile:]
            stage[index * tile : (index + 1) * tile, span] = rms_scale(values, att_gain[...]).astype(BF16)
    for owner in owners:
        hand_over(1, owner).start()

    for copy in own_copies + other_copies + state_copies:
        copy.wait_send()
    if groups > 1:
        swap_kv.wait_send()
        swap_rest.wait_send()
    for which in range(2):
        hand_over(which, owners[0]).wait()
        for owner in owners[1:]:
            hand_over(which, owner).wait_send()
            taken_over(which, owner).wait_recv()


def on_device(
    tokens, norm_gain, rec_query, fwd_gate, bwd_gate, rec_value, gate_leak, log_decay, rec_gain,
    att_query, att_key, att_value, lambdas, att_gain, out_rec, out_att,
):
    ranks = lax.axis_size("sp")
    tp = lax.axis_size("tp")
    local_heads = rec_query.shape[1] // HK
    groups = 2 if local_heads % 2 == 0 and ranks % 2 == 0 else 1
    heads = local_heads // groups
    width = heads * LANES
    slot = lax.axis_index("sp") % groups

    order = (att_key, att_value, att_query, rec_query, fwd_gate, bwd_gate, rec_value)
    length = tokens.shape[0] * tp
    vmem = pl.BlockSpec(memory_space=pltpu.VMEM)
    dma = pltpu.SemaphoreType.DMA
    projected = pl.pallas_call(
        functools.partial(gather_kernel, tp),
        out_shape=[jax.ShapeDtypeStruct((length, weight.shape[1]), BF16) for weight in order],
        in_specs=[vmem] * (2 + len(order)),
        out_specs=[vmem] * len(order),
        scratch_shapes=[
            pltpu.VMEM((length, tokens.shape[1]), BF16),
            dma((tp,)),
            dma((tp // 2,)),
            dma((tp,)),
        ],
        compiler_params=pltpu.CompilerParams(
            collective_id=1, has_side_effects=True, vmem_limit_bytes=40 * 1024 * 1024
        ),
        cost_estimate=pl.CostEstimate(flops=4 * 10**9, bytes_accessed=10**7, transcendentals=0),
    )(tokens, norm_gain.reshape(1, -1), *order)

    positions = (lax.axis_index("sp") * length + jnp.arange(length, dtype=jnp.int32)).astype(F32)
    frequency = THETA ** (-(jnp.arange(AK // 2, dtype=F32) * 2.0 / AK))
    angles = jnp.tile(positions[:, None] * frequency[None, :], (1, LANES // (AK // 2)))
    cosine, sine = jnp.cos(angles), jnp.sin(angles)

    by_head = log_decay.reshape(2, length, groups, heads).transpose(2, 1, 0, 3).reshape(groups, length, 2 * heads)
    own_decay = lax.dynamic_index_in_dim(by_head, slot, 0, keepdims=False)
    if groups > 1:
        swapped = lax.ppermute(
            lax.dynamic_index_in_dim(by_head, groups - 1 - slot, 0, keepdims=False),
            "sp",
            [(i, i + 1 - 2 * (i % 2)) for i in range(ranks)],
        )
        decay = jnp.where(
            slot == 0, jnp.concatenate([own_decay, swapped]), jnp.concatenate([swapped, own_decay])
        )
    else:
        decay = own_decay
    leak = lax.dynamic_index_in_dim(
        gate_leak.reshape(2, groups, heads, HK).transpose(1, 2, 0, 3), slot, 0, keepdims=False
    )
    lam = lax.dynamic_index_in_dim(lambdas.reshape(groups, heads), slot, 0, keepdims=False)
    lam = jnp.broadcast_to(lam[:, None, None], (heads, 1, LANES))

    blocks = ranks // groups
    rows = groups * length
    tile = min(256, length)
    mixers = pl.pallas_call(
        functools.partial(mixer_kernel, ranks, tp, groups, heads, tile),
        out_shape=jax.ShapeDtypeStruct((tp, groups, length // tp, 2 * width), BF16),
        in_specs=[vmem] * 14,
        out_specs=vmem,
        scratch_shapes=[
            pltpu.VMEM((blocks, rows, 2 * width), BF16),
            pltpu.VMEM((rows, 5 * width), BF16),
            pltpu.VMEM((length, 7 * width), BF16),
            pltpu.VMEM((rows, 2 * width), BF16),
            pltpu.VMEM((2, heads, LANES + PAD, LANES), BF16),
            pltpu.VMEM((blocks, heads, LANES + PAD, LANES), BF16),
            pltpu.VMEM((heads, 2, rows, LANES), F32),
            pltpu.VMEM((heads, 2, rows // BLOCK, LANES, LANES), F32),
            pltpu.VMEM((heads, 2, LANES, LANES), F32),
            pltpu.VMEM((rows, width), F32),
            pltpu.VMEM((heads, rows // tile, 2 * tile, LANES), F32),
            pltpu.VMEM((heads, rows // tile, 2 * tile, LANES), F32),
            pltpu.VMEM((heads, rows // tile, 2 * tile, LANES), F32),
            dma((blocks, groups)),
            dma((blocks, groups)),
            dma((2,)),
            dma,
            dma((blocks,)),
            dma((blocks,)),
            dma((2, groups, tp)),
            dma((2, tp, groups)),
        ],
        compiler_params=pltpu.CompilerParams(
            collective_id=0, has_side_effects=True, vmem_limit_bytes=56 * 1024 * 1024
        ),
        cost_estimate=pl.CostEstimate(flops=10**10, bytes_accessed=10**7, transcendentals=10**7),
    )(*projected, cosine, sine, leak, decay, lam, rec_gain.reshape(1, LANES), att_gain.reshape(1, LANES))

    shares = mixers.reshape(tp, groups, length // tp, 2, heads, LANES)
    both = shares.transpose(2, 3, 0, 1, 4, 5).reshape(length // tp, 2, -1)
    result = jnp.dot(both[:, 0], out_rec, preferred_element_type=F32) + jnp.dot(
        both[:, 1], out_att, preferred_element_type=F32
    )
    return result.astype(BF16)


def solution(mesh):
    placed = (
        P(("sp", "tp"), None), P(), P(None, "tp"), P(None, "tp"), P(None, "tp"), P(None, "tp"),
        P(None, "tp"), P(None, "sp", "tp"), P(), P(None, "tp"), P(None, "tp"), P(None, "tp"),
        P("tp"), P(), P(), P(),
    )
    return jax.shard_map(
        on_device, mesh=mesh, in_specs=placed, out_specs=P(("sp", "tp"), None), check_vma=False
    )
```

profile of v0, /device:TPU:0, one launch (start us, length us, event | category | flops | bytes accessed | tf_op | source)
XLA Modules:
  0.0 136.8 jit_solution(5077967458325571512)
XLA Ops:
  0.0 0.8 constant_dynamic-slice_fusion.1
  0.8 3.0 %collective-permute-start = (f32[512,2]{0,1:T(2,128)S(1)}, f32[512,2]{0,1:T(2,128)S(1)}, u32[]{:S(2)}, u32[]{:S(2)}) collective-permute-start(f32[512,2]{0,1:T(2,128)S(1)} %bitcast.45), channel_id=1, source_target_pairs={{0,4},{4,0},{8,12},{12,8},{16,20},{20,16},{24,28},{28,24},{1,5},{5... | collective-permute-start | bytes 12296 | tf_op jit(solution)/shard_map/ppermute | solution.py:460
  3.8 0.3 multiply_sine_fusion
  4.2 1.2 copy-done.1
  5.4 1.2 copy-done.2
  6.6 1.2 copy-done.3
  7.8 1.2 copy-done.4
  9.1 1.2 copy-done.5
  10.3 1.2 copy-done.6
  11.5 1.2 copy-done.7
  12.7 1.0 copy-done.8
  13.8 0.7 copy-done.9
  14.5 17.1 %shard_map.154 = (bf16[512,256]{1,0:T(8,128)(2,1)S(1)}, bf16[512,256]{1,0:T(8,128)(2,1)S(1)}, bf16[512,256]{1,0:T(8,128)(2,1)S(1)}, bf16[512,256]{1,0:T(8,128)(2...) custom-call(bf16[128,2048]{1,0:T(8,128)(2,1)S(1)} %copy-done.8, ...), custom_call_target="tpu_custom_call" | custom-call | flops 4000000000 | bytes 10000000 | tf_op jit(solution)/shard_map/pallas_call | solution.py:435
  31.6 0.7 copy-done.10
  32.3 0.7 copy-done.11
  33.0 0.7 copy-done.12
  33.7 0.7 copy-done.13
  34.4 0.7 copy-done.14
  35.1 0.7 copy-done.15
  35.8 0.7 copy-done.16
  36.5 0.5 dynamic-slice_bitcast_fusion.leak
  37.0 0.6 dynamic-slice.19
  37.7 0.8 copy.40.sine
  38.5 0.8 copy.39.cosine
  39.9 0.9 broadcast_select_fusion.decay
  40.7 1.2 broadcast_in_dim.5.lam
  41.9 88.2 %shard_map.155 = bf16[4,2,128,256]{3,2,1,0:T(8,128)(2,1)} custom-call(bf16[512,256]{1,0:T(8,128)(2,1)} %copy-done.10, bf16[512,256]{1,0:T(8,128)(2,1)} %copy-done.11, bf16[512,256]{1,0:T(8,128)(2,1)} %copy-done.12, bf16[512,256]{1,0:T(8,128)(2,1)} %copy-done.13, bf16[512,256]{1,0:T(8,128)(2,1)} %copy-done.14, bf16[512,256]{1,0:T(8,128)(2,1)} %copy-done.15, ...), custom_call_target="tpu_custom_call" | custom-call | flops 10000000000 | bytes 10000000 | tf_op jit(solution)/shard_map/pallas_call | solution.py:479
  130.1 1.2 reshape.87
  131.3 0.5 copy.41
  131.8 3.1 %fusion.1 = f32[128,2048]{1,0:T(8,128)S(1)} fusion(bf16[1024,2048]{1,0:T(8,128)(2,1)} %param.30, bf16[128,2,1024]{0,2,1:T(8,128)(2,1)S(1)} %bitcast.40), kind=kOutput, calls=%fused_computation.4 | convolution fusion | flops 536870912 | bytes 5505024 | tf_op jit(solution)/shard_map/dot_general | solution.py:515
  134.9 0.4 copy-done.17
  135.2 1.5 %fusion = bf16[128,2048]{1,0:T(8,128)(2,1)} fusion(f32[128,2048]{1,0:T(8,128)S(1)} %fusion.1, bf16[1024,2048]{1,0:T(8,128)(2,1)S(1)} %copy-done.17, bf16[128,2,1024]{0,2,1:T(8,128)(2,1)S(1)} %bitcast.41), kind=kOutput, calls=%fused_computation.1 | convolution fusion | flops 537395200 | bytes 6029312 | tf_op jit(solution)/shard_map/dot_general | solution.py:515
  (31 shorter events, 0.6 us)
Async XLA Ops:
  0.0 36.5 %copy-start = (f32[2,256]{1,0:T(2,128)S(1)}, f32[2,256]{1,0:T(2,128)}, u32[]{:S(2)}) copy-start(f32[2,256]{1,0:T(2,128)} %param.22) | copy-start | bytes 6148
  0.8 38.6 %collective-permute-start = (f32[512,2]{0,1:T(2,128)S(1)}, f32[512,2]{0,1:T(2,128)S(1)}, u32[]{:S(2)}, u32[]{:S(2)}) collective-permute-start(f32[512,2]{0,1:T(2,128)S(1)} %bitcast.45), channel_id=1, source_target_pairs={{0,4},{4,0},{8,12},{12,8},{16,20},{20,16},{24,28},{28,24},{1,5},{5... | collective-permute-start | bytes 12296 | tf_op jit(solution)/shard_map/ppermute | solution.py:460
  4.2 1.2 copy-start.1
  5.4 1.2 copy-start.2
  6.6 1.2 copy-start.3
  7.8 1.2 copy-start.4
  9.1 1.2 copy-start.5
  10.3 1.2 copy-start.6
  11.5 1.2 copy-start.7
  12.7 1.0 copy-start.8
  13.8 0.7 copy-start.9
  14.5 22.5 %copy-start.18 = (f32[2]{0:T(128)S(1)}, f32[2]{0:T(128)}, u32[]{:S(2)}) copy-start(f32[2]{0:T(128)} %param.28) | copy-start | bytes 28
  31.6 0.7 copy-start.10
  32.3 0.7 copy-start.11
  33.0 0.7 copy-start.12
  33.7 0.7 copy-start.13
  34.4 0.7 copy-start.14
  35.1 0.7 copy-start.15
  35.7 0.7 copy-start.16
  131.8 3.5 %copy-start.17 = (bf16[1024,2048]{1,0:T(8,128)(2,1)S(1)}, bf16[1024,2048]{1,0:T(8,128)(2,1)}, u32[]{:S(2)}) copy-start(bf16[1024,2048]{1,0:T(8,128)(2,1)} %param.31) | copy-start | bytes 12582916
where the time goes:
time: 137 us
  Pallas kernels  105 us (77%)
  local copies, waits for them, and re-layouts  22.5 us (16%)
  matrix products  4.62 us (3%)
  starting transfers between devices  3.03 us (2%)
    pallas_call x1, Pallas kernels, on_device(): pl.pallas_call(functools.partial(mixer_kernel, ranks, tp, groups, heads,...  88.2 us
    pallas_call x1, Pallas kernels, on_device(): pl.pallas_call(functools.partial(gather_kernel, tp), out_shape=[jax.Shape...  17.1 us
    unnamed x40, local copies, waits for them, and re-layouts  15.5 us
    dot_general x1, matrix products, on_device(): jnp.dot(both[:, 0], out_rec, preferred_element_type=F32)  3.08 us
    ppermute x1, starting transfers between devices, on_device(): lax.ppermute(lax.dynamic_index_in_dim(by_head, groups - 1 - slot, 0, keep...  3.03 us
  transfers between devices with their start and end apart: 1, of which 0 were waited for; matrix products, arithmetic and copies ran while one was open for 2% of the time, Pallas kernels for 12%

commit v1 on v0

--- a/solution.py
+++ b/solution.py
@@ -2,6 +2,7 @@
 
 import jax
 import jax.numpy as jnp
+import numpy as np
 from jax import lax
 from jax.experimental import pallas as pl
 from jax.experimental.pallas import tpu as pltpu
@@ -416,7 +417,7 @@
             taken_over(which, owner).wait_recv()
 
 
-def on_device(
+def on_device_general(
     tokens, norm_gain, rec_query, fwd_gate, bwd_gate, rec_value, gate_leak, log_decay, rec_gain,
     att_query, att_key, att_value, lambdas, att_gain, out_rec, out_att,
 ):
@@ -518,6 +519,662 @@
     return result.astype(BF16)
 
 
+def fused_kernel(
+    ranks, tp, heads, planes,
+    tokens_in, norm_in, w_key, w_value, w_query, w_rq, w_fwd, w_bwd, w_rv, leak_in, decay_in, rec_gain_in,
+    lam_in, att_gain_in, out_rec_in, out_att_in, rotary_in,
+    out,
+    tokens, gain, weights, leak, decay, rec_gain, lam, att_gain, w_out_rec, w_out_att, rotary,
+    held, cosine, sine, lam_own, lam_pair, stage, land, recp, cum_reads, facts, adds, rec_sum,
+    state, fade, pair_out, pair_in, plane_out, plane_in, plane_sum, next_out, next_in, before_block,
+    rec_stage, rec_all, score_a, score_b, top_a, top_b, acc, peak, att_stage, att_all, total,
+    in_sem, across_send, across_recv, core_send, core_recv, lam_send, lam_recv,
+    qkv_send, qkv_recv, side_send, side_recv, near_send, near_recv,
+    pair_send, pair_recv, plane_send, plane_recv, next_send, next_recv,
+    rec_send, rec_recv, att_send, att_recv,
+):
+    sp = lax.axis_index("sp")
+    me = lax.axis_index("tp")
+    x = lax.rem(sp, 2)
+    z = lax.div(sp, 2)
+    core = lax.rem(me, 2)
+    y = lax.div(me, 2)
+    piece = tokens.shape[0]
+    half = piece // 2
+    length = piece * tp
+    width = heads * LANES
+    here = {"sp": sp, "tp": me}
+    partner = {"tp": y * 2 + 1 - core}
+    opposite = {"tp": (1 - y) * 2 + core}
+    beside = {"sp": z * 2 + 1 - x}
+
+    sources = (
+        tokens_in, norm_in, rotary_in, lam_in, w_key, w_value, w_query, w_rq, w_fwd, w_bwd, w_rv,
+        leak_in, decay_in, rec_gain_in, att_gain_in, out_rec_in, out_att_in,
+    )
+    targets = (
+        tokens, gain, rotary, lam, *(weights.at[i] for i in range(7)),
+        leak, decay, rec_gain, att_gain, w_out_rec, w_out_att,
+    )
+    fetches = [pltpu.make_async_copy(a, b, in_sem.at[i]) for i, (a, b) in enumerate(zip(sources, targets))]
+    for fetch in fetches:
+        fetch.start()
+
+    barrier = pltpu.get_barrier_semaphore()
+    for dz in range(planes):
+        for dt in range(tp):
+            if dz or dt:
+                to = {"sp": lax.rem(z + dz, planes) * 2 + x, "tp": lax.rem(me + dt, tp)}
+                pl.semaphore_signal(barrier, inc=1, device_id=to)
+    pl.semaphore_signal(barrier, inc=1, device_id=beside)
+
+    def remote(source, target, send, recv, to):
+        return pltpu.make_async_remote_copy(
+            src_ref=source, dst_ref=target, send_sem=send, recv_sem=recv, device_id=to
+        )
+
+    fetches[2].wait()
+    lane = lax.broadcasted_iota(jnp.int32, (piece, LANES), 1)
+    low_half = lax.rem(lane, AK) < AK // 2
+    for t in range(tp):
+        first = 2 * piece + sp * tp + t
+        cos_base = rotary[pl.ds(first, 1), :]
+        sin_base = rotary[pl.ds(first + ranks * tp, 1), :]
+        cos_row, sin_row = rotary[:piece, :], rotary[piece : 2 * piece, :]
+        cosine[t * piece : (t + 1) * piece, :] = cos_base * cos_row - sin_base * sin_row
+        turned = sin_base * cos_row + cos_base * sin_row
+        sine[t * piece : (t + 1) * piece, :] = jnp.where(low_half, -turned, turned)
+
+    def rows_of_piece(t, begin, count):
+        return held.at[pl.ds(pl.multiple_of(t * piece + begin, half), count)]
+
+    def across(part):
+        rows = rows_of_piece(me, part * half, half)
+        return remote(rows, rows, across_send.at[part], across_recv.at[part], opposite)
+
+    def from_across(part):
+        rows = rows_of_piece((1 - y) * 2 + core, part * half, half)
+        return remote(rows, rows, across_send.at[part], across_recv.at[part], opposite)
+
+    def to_core(t, slot, begin, count):
+        rows = rows_of_piece(t, begin, count)
+        return remote(rows, rows, core_send.at[slot], core_recv.at[slot], partner)
+
+    fetches[0].wait()
+    fetches[1].wait()
+    for part in range(2):
+        rows = tokens[part * half : (part + 1) * half, :].astype(F32)
+        held[pl.ds(pl.multiple_of(me * piece + part * half, half), half), :] = rms_scale(rows, gain[...]).astype(BF16)
+        if part == 0:
+            pl.semaphore_wait(barrier, planes * tp)
+        across(part).start()
+    to_core(me, 0, 0, piece).start()
+    fetches[3].wait()
+    for i in range(heads):
+        lam_own[i] = jnp.broadcast_to(lam[:, i : i + 1], (8, LANES))
+    lam_copy = remote(lam_own, lam_pair, lam_send, lam_recv, partner)
+    lam_copy.start()
+
+    def rotated(wide, at):
+        turned = jnp.where(
+            jnp.concatenate([low_half] * 2, axis=0),
+            pltpu.roll(wide, LANES - AK // 2, 1), pltpu.roll(wide, AK // 2, 1),
+        )
+        return wide * cosine[at, :] + turned * sine[at, :]
+
+    def phase_rows(phase):
+        owner = y if phase == 0 else 1 - y
+        return pl.ds(pl.multiple_of(owner * 2 * piece, 2 * piece), 2 * piece)
+
+    def project(phase, index):
+        return jnp.dot(held[phase_rows(phase), :], weights[index], preferred_element_type=F32)
+
+    def qkv_target(i, c):
+        return core * heads + i, c
+
+    def qkv_copy(phase, i, c):
+        return remote(
+            stage.at[phase, i, c], land.at[0, phase, z], qkv_send.at[phase, i, c], qkv_recv.at[phase, z],
+            {"sp": (core * heads + i) * 2 + x, "tp": y * 2 + c},
+        )
+
+    def qkv_is_own(i, c):
+        return jnp.logical_and(core * heads + i == z, core == c)
+
+    def attention_inputs(phase):
+        at = phase_rows(phase)
+        if phase == 0:
+            fetches[4].wait()
+        keys = project(phase, 0).astype(BF16).astype(F32)
+        if phase == 0:
+            fetches[5].wait()
+        values = project(phase, 1).astype(BF16).astype(F32)
+        if phase == 0:
+            fetches[6].wait()
+        queries = project(phase, 2).astype(BF16).astype(F32)
+        for i in range(heads):
+            span = slice(i * LANES, (i + 1) * LANES)
+            key = rotated(keys[:, span], at).astype(BF16)
+            value = values[:, span].T.astype(BF16)
+            query = (rotated(queries[:, span], at) * AK ** (-0.5)).astype(BF16)
+            for c in range(2):
+                part = slice(c * piece, (c + 1) * piece)
+                stage[phase, i, c, :piece, :] = key[part]
+                stage[phase, i, c, piece : 2 * piece, :] = value[:, part]
+                stage[phase, i, c, 2 * piece :, :] = query[part]
+        for i in range(heads):
+            for c in range(2):
+                own = qkv_is_own(i, c)
+
+                @pl.when(own)
+                def _():
+                    pltpu.make_async_copy(
+                        stage.at[phase, i, c], land.at[0, phase, z], qkv_recv.at[phase, z]
+                    ).start()
+
+                @pl.when(jnp.logical_not(own))
+                def _():
+                    qkv_copy(phase, i, c).start()
+
+    def recurrence_inputs(phase):
+        for i in range(4):
+            if phase == 0:
+                fetches[7 + i].wait()
+            recp[i, phase_rows(phase), :] = project(phase, 3 + i).astype(BF16)
+
+    def plane_at(k):
+        return (z, z + 1 - 2 * lax.rem(z, 2), lax.rem(z + 2, 4), planes - 1 - z)[k] if planes == 4 else lax.rem(z + k, planes)
+
+    def kv_of(origin, phase, plane):
+        return land.at[origin, phase, plane, : 2 * piece]
+
+    def to_side(phase, plane):
+        return remote(
+            kv_of(0, phase, plane), kv_of(2, phase, plane),
+            side_send.at[phase, plane], side_recv.at[phase, plane], beside,
+        )
+
+    def to_near(origin, phase, plane):
+        return remote(
+            kv_of(origin, phase, plane), kv_of(origin + 1, phase, plane),
+            near_send.at[origin // 2, phase, plane], near_recv.at[origin // 2, phase, plane], partner,
+        )
+
+    def relay_plane(phase, k):
+        plane = plane_at(k)
+        remote(
+            land.at[0, phase, plane], land.at[0, phase, plane],
+            qkv_send.at[phase, 0, 0], qkv_recv.at[phase, plane], partner,
+        ).wait_recv()
+        to_side(phase, plane).start()
+        to_near(0, phase, plane).start()
+
+    def relay_side(phase, k):
+        plane = plane_at(k)
+        to_side(phase, plane).wait_recv()
+        to_near(2, phase, plane).start()
+
+    def settle(phase):
+        for k in range(planes):
+            for origin in (0, 2):
+                to_near(origin, phase, plane_at(k)).wait_recv()
+
+    row_at = lax.broadcasted_iota(jnp.int32, (BLOCK, 3 * BLOCK), 0)
+    col_at = lax.rem(lax.broadcasted_iota(jnp.int32, (BLOCK, 3 * BLOCK), 1), BLOCK)
+    triangles = (jnp.where(row_at >= col_at, 1.0, 0.0).astype(BF16), jnp.where(row_at <= col_at, 1.0, 0.0).astype(BF16))
+    row_in = lax.broadcasted_iota(jnp.int32, (BLOCK, BLOCK), 0)
+    col_in = lax.broadcasted_iota(jnp.int32, (BLOCK, BLOCK), 1)
+    earlier = (row_in >= col_in, row_in <= col_in)
+    ends = (BLOCK - 1, 0)
+    middles = (BLOCK // 2 - 1, BLOCK // 2)
+    blocks = length // BLOCK
+    spans = [slice(h * LANES, (h + 1) * LANES) for h in range(heads)]
+
+    def within_block(b):
+        at = pl.ds(pl.multiple_of(b * BLOCK, BLOCK), BLOCK)
+        queries = jax.nn.silu(recp[0, at, :].astype(F32))
+        values = recp[3, at, :]
+        scores, tails = [], []
+        for d in range(2):
+            keys = leak[d : d + 1, :] * jax.nn.sigmoid(-recp[1 + d, at, :].astype(F32))
+            added = jnp.concatenate(
+                [jnp.broadcast_to(decay[d, at, h : h + 1], (BLOCK, LANES)) for h in range(heads)], axis=1
+            )
+            logs = jnp.log1p(-keys) + added
+            coarse = logs.astype(BF16)
+            rest = logs - coarse.astype(F32)
+            fine = rest.astype(BF16)
+            finest = (rest - fine.astype(F32)).astype(BF16)
+            cum = jnp.dot(
+                triangles[d], jnp.concatenate([coarse, fine, finest], axis=0), preferred_element_type=F32
+            )
+            middle = cum[middles[d] : middles[d] + 1, :]
+            last = cum[ends[d] : ends[d] + 1, :]
+            reads = (queries * jnp.exp(cum - middle)).astype(BF16)
+            writes = (keys * jnp.exp(middle - cum)).astype(BF16)
+            tails.append((keys * jnp.exp(last - cum)).astype(BF16))
+            carried = (queries * jnp.exp(cum)).astype(BF16)
+            facts[b, d] = jnp.broadcast_to(jnp.exp(last), (8, width))
+            scores.append([jnp.where(earlier[d], dot_t(reads[:, s], writes[:, s]), 0.0) for s in spans])
+            for h in range(heads):
+                cum_reads[h, at, d * LANES : (d + 1) * LANES] = carried[:, spans[h]]
+        for h in range(heads):
+            both = (scores[0][h] + scores[1][h]).astype(BF16)
+            rec_sum[at, spans[h]] = jnp.dot(both, values[:, spans[h]], preferred_element_type=F32)
+            adds[b, h] = dot_0(
+                values[:, spans[h]], jnp.concatenate([tails[0][:, spans[h]], tails[1][:, spans[h]]], axis=1)
+            )
+
+    def within_phase(phase):
+        owner = y if phase == 0 else 1 - y
+        count = blocks // 2
+
+        def some(j, carry):
+            within_block(owner * count + 2 * j)
+            within_block(owner * count + 2 * j + 1)
+            return carry
+
+        lax.fori_loop(0, count // 2, some, 0)
+
+    def order(d):
+        return range(blocks) if d == 0 else range(blocks - 1, -1, -1)
+
+    def half_of(d):
+        return slice(d * LANES, (d + 1) * LANES)
+
+    first_row = lax.broadcasted_iota(jnp.int32, (PAD, LANES), 0) == 0
+
+    def pack(target, moved, factor):
+        target[:LANES, :] = moved.astype(BF16)
+        wide = jnp.broadcast_to(factor, (PAD, LANES))
+        coarse = wide.astype(BF16).astype(F32)
+        target[LANES:, :] = jnp.where(first_row, coarse, wide - coarse).astype(BF16)
+
+    def unpack(source):
+        last = source[LANES:, :].astype(F32)
+        return source[:LANES, :].astype(F32), last[0:1] + last[1:2]
+
+    def local_states():
+        for h in range(heads):
+            for d in range(2):
+                moved = jnp.zeros((LANES, LANES), F32)
+                factor = jnp.ones((1, LANES), F32)
+                for b in order(d):
+                    step = facts[b, d, 0:1, spans[h]]
+                    moved = moved * step + adds[b, h, :, half_of(d)]
+                    factor = factor * step
+                state[d, h] = moved
+                fade[d, h] = jnp.broadcast_to(factor, (8, LANES))
+                pack(pair_out.at[d, h], moved, factor)
+
+    pair_copy = remote(pair_out, pair_in, pair_send, pair_recv, beside)
+
+    def pair_states():
+        pair_copy.wait_recv()
+        for d in range(2):
+            mine, factor = state[d, x], fade[d, x][0:1]
+            other, other_factor = unpack(pair_in.at[d, x])
+            joined = jnp.where(x == d, mine * other_factor + other, other * factor + mine)
+            pack(plane_out.at[d], joined, factor * other_factor)
+        for dz in range(1, planes):
+            to_plane(lax.rem(z + dz, planes)).start()
+
+    def to_plane(target):
+        return remote(
+            plane_out.at[jnp.where(target > z, 0, 1)], plane_in.at[z],
+            plane_send.at[target], plane_recv.at[z], {"sp": target * 2 + x},
+        )
+
+    def from_plane(source):
+        return remote(
+            plane_out.at[0], plane_in.at[source],
+            plane_send.at[source], plane_recv.at[source], {"sp": source * 2 + x},
+        )
+
+    next_copy = remote(next_out, next_in, next_send, next_recv, beside)
+
+    def plane_states():
+        plane_sum[...] = jnp.zeros_like(plane_sum)
+
+        def fold(d):
+            def one(step, carry):
+                plane = step if d == 0 else planes - 1 - step
+                from_plane(plane).wait_recv()
+                moved, factor = unpack(plane_in.at[plane])
+                plane_sum[d] = plane_sum[d] * factor + moved
+                return carry
+
+            return one
+
+        lax.fori_loop(0, z, fold(0), 0)
+        lax.fori_loop(0, planes - 1 - z, fold(1), 0)
+        next_out[...] = plane_sum[...].astype(BF16)
+        next_copy.start()
+
+    def second_pass():
+        next_copy.wait_recv()
+        for h in range(heads):
+            for d in range(2):
+                entering = jnp.where(x == h, plane_sum[d], next_in[d].astype(F32))
+                other, other_factor = unpack(pair_in.at[d, h])
+                running = jnp.where(x == d, entering, entering * other_factor + other)
+                for b in order(d):
+                    before_block[b, h, :, half_of(d)] = running.astype(BF16)
+                    running = running * facts[b, d, 0:1, spans[h]] + adds[b, h, :, half_of(d)]
+            for b in range(blocks):
+                at = slice(b * BLOCK, (b + 1) * BLOCK)
+                whole = rec_sum[at, spans[h]] + dot_t(cum_reads[h, at, :], before_block[b, h])
+                rec_stage[at, spans[h]] = rms_scale(whole, rec_gain[...]).astype(BF16)
+        for dt in range(tp):
+            rec_copy(dt).start()
+
+    def rec_copy(dt):
+        t = lax.rem(me + dt, tp)
+        source = rec_stage.at[pl.ds(pl.multiple_of(t * piece, piece), piece)]
+        if dt == 0:
+            return pltpu.make_async_copy(source, rec_all.at[me], rec_recv.at[me])
+        return remote(source, rec_all.at[me], rec_send.at[dt], rec_recv.at[me], {"tp": t})
+
+    def rec_arrival(dt):
+        t = lax.rem(me + dt, tp)
+        return remote(rec_all.at[t], rec_all.at[t], rec_send.at[dt], rec_recv.at[t], {"tp": t})
+
+    acc[...] = jnp.zeros_like(acc)
+    peak[...] = jnp.full_like(peak, -jnp.inf)
+    sub = 2 * piece
+    ones = jnp.ones((PAD, sub), BF16)
+    low_map = lane < AK
+    sub_count = 4 * planes * piece // sub
+
+    def key_block(phase, u, part):
+        block = 2 * u + part
+        return block // planes, phase, block % planes
+
+    def attend_step(phase, made, made_score, made_top, used, used_score):
+        if made is not None:
+            q_phase, tile = made
+            query = land[0, q_phase, tile, 2 * piece :, :]
+            none = jnp.zeros_like(query)
+            both = jnp.concatenate([jnp.where(low_map, query, none), jnp.where(low_map, none, query)], axis=0)
+            top = None
+        if used is not None:
+            q_phase_used, tile_used, used_top = used
+            slot = q_phase_used * planes + tile_used
+            before = peak[slot][0:1]
+            now = jnp.maximum(before, jnp.max(used_top[...], axis=0, keepdims=True))
+            mixed = acc[slot] * jnp.exp(before - now)
+        for u in range(sub_count):
+            at = slice(u * sub, (u + 1) * sub)
+            if made is not None:
+                keys = jnp.concatenate(
+                    [land[(*key_block(phase, u, part), slice(0, piece))] for part in range(2)], axis=0
+                )
+                scores = dot_t(keys, both)
+                made_score[at, :] = scores
+                high = jnp.max(scores.reshape(sub // 8, 8, 2 * piece), axis=0)
+                top = high if top is None else jnp.maximum(top, high)
+            if used is not None:
+                expo = jnp.exp(used_score[at, :] - now).astype(BF16)
+                values = jnp.concatenate(
+                    [land[(*key_block(phase, u, part), slice(piece, 2 * piece))] for part in range(2)], axis=1
+                )
+                values = jnp.concatenate([values, ones], axis=0)
+                mixed = mixed + jnp.dot(values, expo, preferred_element_type=F32)
+        if used is not None:
+            acc[slot] = mixed
+            peak[slot] = jnp.broadcast_to(now, (8, 2 * piece))
+        if made is not None:
+            made_top[...] = top
+
+    def attend(q_phase, phase, after):
+        attend_step(phase, (q_phase, 0), score_a, top_a, None, None)
+        buffers = ((score_a, top_a), (score_b, top_b))
+        for tile in range(1, planes + 1):
+            used_score, used_top = buffers[(tile - 1) % 2]
+            made_score, made_top = buffers[tile % 2]
+            made = (q_phase, tile) if tile < planes else None
+            attend_step(phase, made, made_score, made_top, (q_phase, tile - 1, used_top), used_score)
+            after(tile - 1)
+
+    def att_target(q_phase, tile):
+        owner = y if q_phase == 0 else 1 - y
+        return owner, {"sp": tile * 2 + x, "tp": owner * 2 + core}
+
+    def att_copy(q_phase, tile):
+        owner, to = att_target(q_phase, tile)
+        return remote(
+            att_stage.at[q_phase, tile], att_all.at[y * planes + z],
+            att_send.at[q_phase, tile], att_recv.at[y * planes + z], to,
+        )
+
+    def finish(q_phase, tile):
+        whole = acc[q_phase * planes + tile]
+        ratio = whole[:LANES] / whole[LANES : LANES + 1]
+        weight = jnp.where(core == lax.div(z, heads), lam_own[lax.rem(z, heads)], lam_pair[lax.rem(z, heads)])[0:1]
+        values = ratio[:, :piece] - weight * ratio[:, piece:]
+        scale = lax.rsqrt(jnp.mean(values * values, axis=0, keepdims=True) + EPS)
+        att_stage[q_phase, tile] = ((values * scale).T * att_gain[...]).astype(BF16)
+        if q_phase == 0:
+            own = tile == z
+
+            @pl.when(own)
+            def _():
+                pltpu.make_async_copy(
+                    att_stage.at[q_phase, tile], att_all.at[y * planes + z], att_recv.at[y * planes + z]
+                ).start()
+
+            @pl.when(jnp.logical_not(own))
+            def _():
+                att_copy(q_phase, tile).start()
+        else:
+            att_copy(q_phase, tile).start()
+
+    def att_arrival(index):
+        return remote(att_all.at[index], att_all.at[index], att_send.at[0, 0], att_recv.at[index], partner)
+
+    def nothing(tile):
+        pass
+
+    columns = min(512, out.shape[1])
+
+    to_core(y * 2 + 1 - core, 0, 0, piece).wait_recv()
+    attention_inputs(0)
+    recurrence_inputs(0)
+    for i in range(11, 15):
+        fetches[i].wait()
+    relay_plane(0, 0)
+    within_phase(0)
+    relay_plane(0, 1)
+    for part in range(2):
+        from_across(part).wait_recv()
+        to_core((1 - y) * 2 + core, 1 + part, part * half, half).start()
+    relay_side(0, 0)
+    for part in range(2):
+        to_core((1 - y) * 2 + 1 - core, 1 + part, part * half, half).wait_recv()
+    attention_inputs(1)
+    relay_plane(0, 2)
+    relay_plane(0, 3)
+    relay_side(0, 1)
+    recurrence_inputs(1)
+    within_phase(1)
+    local_states()
+    pair_copy.start()
+    relay_plane(1, 0)
+    relay_side(0, 2)
+    relay_side(0, 3)
+    settle(0)
+    lam_copy.wait_recv()
+
+    def while_early(tile):
+        if tile == 0:
+            pair_states()
+            relay_plane(1, 1)
+        if tile == 1:
+            relay_plane(1, 2)
+            relay_side(1, 0)
+        if tile == 2:
+            relay_plane(1, 3)
+
+    attend(0, 0, while_early)
+
+    def while_later(tile):
+        if tile == 0:
+            relay_side(1, 1)
+            plane_states()
+        if tile == 1:
+            relay_side(1, 2)
+        if tile == 2:
+            relay_side(1, 3)
+
+    attend(1, 0, while_later)
+    second_pass()
+    settle(1)
+    attend(0, 1, functools.partial(finish, 0))
+    fetches[15].wait()
+    fetches[16].wait()
+    for dt in range(tp):
+        rec_arrival(dt).wait_recv()
+    rec_rows = jnp.concatenate([rec_all[t] for t in range(tp)], axis=1)
+    for n in range(0, out.shape[1], columns):
+        total[:, n : n + columns] = jnp.dot(rec_rows, w_out_rec[:, n : n + columns], preferred_element_type=F32)
+    attend(1, 1, functools.partial(finish, 1))
+    for index in range(2 * planes):
+        att_arrival(index).wait_recv()
+    att_rows = jnp.concatenate([att_all[i] for i in range(2 * planes)], axis=1)
+    for n in range(0, out.shape[1], columns):
+        out[:, n : n + columns] = (
+            total[:, n : n + columns]
+            + jnp.dot(att_rows, w_out_att[:, n : n + columns], preferred_element_type=F32)
+        ).astype(BF16)
+
+    for part in range(2):
+        across(part).wait_send()
+        to_core((1 - y) * 2 + core, 1 + part, part * half, half).wait_send()
+    to_core(me, 0, 0, piece).wait_send()
+    lam_copy.wait_send()
+    for phase in range(2):
+        for i in range(heads):
+            for c in range(2):
+
+                @pl.when(jnp.logical_not(qkv_is_own(i, c)))
+                def _():
+                    qkv_copy(phase, i, c).wait_send()
+
+        for k in range(planes):
+            to_side(phase, plane_at(k)).wait_send()
+            to_near(0, phase, plane_at(k)).wait_send()
+            to_near(2, phase, plane_at(k)).wait_send()
+    pair_copy.wait_send()
+    next_copy.wait_send()
+    for dz in range(1, planes):
+        to_plane(lax.rem(z + dz, planes)).wait_send()
+    for dt in range(1, tp):
+        rec_copy(dt).wait_send()
+    for tile in range(planes):
+
+        @pl.when(tile != z)
+        def _():
+            att_copy(0, tile).wait_send()
+
+        att_copy(1, tile).wait_send()
+
+
+def rotary_table(piece, pieces):
+    frequency = THETA ** (-(np.arange(LANES) % (AK // 2)) * 2.0 / AK)
+    inside = np.arange(piece)[:, None] * frequency[None, :]
+    base = (np.arange(pieces) * piece)[:, None] * frequency[None, :]
+    return np.concatenate([np.cos(inside), np.sin(inside), np.cos(base), np.sin(base)]).astype(np.float32)
+
+
+def on_device(
+    tokens, norm_gain, rec_query, fwd_gate, bwd_gate, rec_value, gate_leak, log_decay, rec_gain,
+    att_query, att_key, att_value, lambdas, att_gain, out_rec, out_att,
+):
+    ranks = lax.axis_size("sp")
+    tp = lax.axis_size("tp")
+    heads = rec_query.shape[1] // HK
+    planes = ranks // 2
+    piece, model = tokens.shape
+    if tp != 4 or planes != 2 * heads or planes != 4 or piece != LANES:
+        return on_device_general(
+            tokens, norm_gain, rec_query, fwd_gate, bwd_gate, rec_value, gate_leak, log_decay, rec_gain,
+            att_query, att_key, att_value, lambdas, att_gain, out_rec, out_att,
+        )
+    length = piece * tp
+    width = heads * LANES
+    blocks = length // BLOCK
+    keys = 4 * planes * piece
+    anywhere = pl.BlockSpec(memory_space=pl.ANY)
+    dma = pltpu.SemaphoreType.DMA
+    vmem = pltpu.VMEM
+    table = jnp.asarray(rotary_table(piece, ranks * tp))
+    return pl.pallas_call(
+        functools.partial(fused_kernel, ranks, tp, heads, planes),
+        out_shape=jax.ShapeDtypeStruct((piece, model), BF16),
+        in_specs=[anywhere] * 17,
+        out_specs=pl.BlockSpec(memory_space=pltpu.VMEM),
+        scratch_shapes=[
+            vmem((piece, model), BF16),
+            vmem((1, model), F32),
+            vmem((7, model, width), BF16),
+            vmem((2, width), F32),
+            vmem((2, length, heads), F32),
+            vmem((1, LANES), F32),
+            vmem((1, heads), F32),
+            vmem((1, LANES), F32),
+            vmem(out_rec.shape, BF16),
+            vmem(out_att.shape, BF16),
+            vmem(table.shape, F32),
+            vmem((length, model), BF16),
+            vmem((length, LANES), F32),
+            vmem((length, LANES), F32),
+            vmem((heads, 8, LANES), F32),
+            vmem((heads, 8, LANES), F32),
+            vmem((2, heads, 2, 3 * piece, LANES), BF16),
+            vmem((4, 2, planes, 3 * piece, LANES), BF16),
+            vmem((4, length, width), BF16),
+            vmem((heads, length, 2 * LANES), BF16),
+            vmem((blocks, 2, 8, width), F32),
+            vmem((blocks, heads, LANES, 2 * LANES), F32),
+            vmem((length, width), F32),
+            vmem((2, heads, LANES, LANES), F32),
+            vmem((2, heads, 8, LANES), F32),
+            vmem((2, heads, LANES + PAD, LANES), BF16),
+            vmem((2, heads, LANES + PAD, LANES), BF16),
+            vmem((2, LANES + PAD, LANES), BF16),
+            vmem((planes, LANES + PAD, LANES), BF16),
+            vmem((2, LANES, LANES), F32),
+            vmem((2, LANES, LANES), BF16),
+            vmem((2, LANES, LANES), BF16),
+            vmem((blocks, heads, LANES, 2 * LANES), BF16),
+            vmem((length, width), BF16),
+            vmem((tp, piece, width), BF16),
+            vmem((keys, 2 * piece), F32),
+            vmem((keys, 2 * piece), F32),
+            vmem((8, 2 * piece), F32),
+            vmem((8, 2 * piece), F32),
+            vmem((2 * planes, LANES + PAD, 2 * piece), F32),
+            vmem((2 * planes, 8, 2 * piece), F32),
+            vmem((2, planes, piece, LANES), BF16),
+            vmem((2 * planes, piece, LANES), BF16),
+            vmem((piece, model), F32),
+            dma((17,)), dma((2,)), dma((2,)), dma((3,)), dma((3,)), dma, dma,
+            dma((2, heads, 2)), dma((2, planes)), dma((2, planes)), dma((2, planes)),
+            dma((2, 2, planes)), dma((2, 2, planes)),
+            dma, dma, dma((planes,)), dma((planes,)), dma, dma,
+            dma((tp,)), dma((tp,)), dma((2, planes)), dma((2 * planes,)),
+        ],
+        compiler_params=pltpu.CompilerParams(
+            collective_id=2, has_side_effects=True, vmem_limit_bytes=60 * 1024 * 1024
+        ),
+        cost_estimate=pl.CostEstimate(flops=10**10, bytes_accessed=10**7, transcendentals=10**7),
+    )(
+        tokens, norm_gain.reshape(1, -1), att_key, att_value, att_query, rec_query, fwd_gate, bwd_gate, rec_value,
+        gate_leak, log_decay, rec_gain.reshape(1, LANES), lambdas.reshape(1, heads), att_gain.reshape(1, LANES),
+        out_rec, out_att, table,
+    )
+
+
 def solution(mesh):
     placed = (
         P(("sp", "tp"), None), P(), P(None, "tp"), P(None, "tp"), P(None, "tp"), P(None, "tp"),

time: 137 us -> 57.2 us (0.42)
  Pallas kernels: 105 us -> 53.4 us
  local copies, waits for them, and re-layouts: 22.5 us -> 3.6 us
  matrix products: 4.62 us -> 0 us
  starting transfers between devices: 3.03 us -> 0 us
    pallas_call x2 -> x1, Pallas kernels: 105 us -> 53.4 us  [on_device(): pl.pallas_call(functools.partial(fused_kernel, ranks, tp, heads, planes),...]
    unnamed x40 -> x2, local copies, waits for them, and re-layouts: 15.5 us -> 3.6 us
    dot_general x2 -> x0, matrix products: 4.62 us -> none  [the longest x1 3.08 us: on_device(): jnp.dot(both[:, 0], out_rec, preferred_element_type=F32)]
    ppermute x1 -> x0, starting transfers between devices: 3.03 us -> none  [on_device(): lax.ppermute(lax.dynamic_index_in_dim(by_head, groups - 1 - slot, 0, keep...]
    reshape x2 -> x0, local copies, waits for them, and re-layouts: 1.65 us -> none  [on_device(): shares = mixers.reshape(tp, groups, length // tp, 2, heads, LANES)]
    another operation x4 -> x0, local copies, waits for them, and re-layouts: 1.46 us -> none
  transfers between devices with their start and end apart: 1 -> 0, of which waited for: 0 -> 0; matrix products, arithmetic and copies ran while one was open for 2% -> 0% of each run, Pallas kernels for 12% -> 0%
where the time goes in v1:
time: 57.2 us; the launch traced here: 57 us
  Pallas kernels  53.4 us (93%)
  local copies, waits for them, and re-layouts  3.6 us (6%)
    pallas_call x1, Pallas kernels, on_device(): pl.pallas_call(functools.partial(fused_kernel, ranks, tp, heads, planes),...  53.4 us
    unnamed x2, local copies, waits for them, and re-layouts  3.6 us

profile of v1, /device:TPU:0, one launch (start us, length us, event | category | flops | bytes accessed | tf_op | source)
XLA Modules:
  0.0 57.0 jit_solution(9154309634408025684)
XLA Ops:
  0.0 1.7 %copy.18.decay_in = f32[2,512,2]{2,1,0:T(8,128)} copy(f32[2,512,2]{1,2,0:T(2,128)} %param.24) | data formatting | bytes 16384 | tf_op args[7]
  1.7 53.4 %shard_map.163 = bf16[128,2048]{1,0:T(8,128)(2,1)} custom-call(bf16[128,2048]{1,0:T(8,128)(2,1)} %tokens_in.1, f32[1,2048]{1,0:T(1,128)} %bitcast.4, bf16[2048,256]{1,0:T(8,128)(2,1)} %w_key.1, bf16[2048,256]{1,0:T(8,128)(2,1)} %w_value.1, bf16[2048,256]{1,0:T(8,128)(2,1)} %w_query.1, bf16[2048,256]{1,0:T(8,128)(2,1)} %w_rq.1, bf16[2048,256]{1,0:T(8,128)(2,1)} %w_fwd.1, ...), custom_call_target="tpu_custom_call" | custom-call | flops 10000000000 | bytes 10000000 | tf_op jit(solution)/shard_map/pallas_call | solution.py:1111
  55.1 1.9 %copy.20 = bf16[128,2048]{1,0:T(8,128)(2,1)} copy(bf16[128,2048]{1,0:T(8,128)(2,1)} %shard_map.163) | data formatting | bytes 1048576

commit v2 on v1

--- a/solution.py
+++ b/solution.py
@@ -524,12 +524,12 @@
     tokens_in, norm_in, w_key, w_value, w_query, w_rq, w_fwd, w_bwd, w_rv, leak_in, decay_in, rec_gain_in,
     lam_in, att_gain_in, out_rec_in, out_att_in, rotary_in,
     out,
-    tokens, gain, weights, leak, decay, rec_gain, lam, att_gain, w_out_rec, w_out_att, rotary,
-    held, cosine, sine, lam_own, lam_pair, stage, land, recp, cum_reads, facts, adds, rec_sum,
+    tokens, gain, weights, leak, decay, decay_rows, rec_gain, lam, att_gain, w_out_rec, w_out_att, rotary,
+    held, cosine, sine, lam_own, lam_pair, stage_kv, stage_q, kv, query, recp, cum_reads, facts, adds, rec_sum,
     state, fade, pair_out, pair_in, plane_out, plane_in, plane_sum, next_out, next_in, before_block,
     rec_stage, rec_all, score_a, score_b, top_a, top_b, acc, peak, att_stage, att_all, total,
     in_sem, across_send, across_recv, core_send, core_recv, lam_send, lam_recv,
-    qkv_send, qkv_recv, side_send, side_recv, near_send, near_recv,
+    kv_send, kv_recv, q_send, q_recv, side_send, side_recv, near_send, near_recv,
     pair_send, pair_recv, plane_send, plane_recv, next_send, next_recv,
     rec_send, rec_recv, att_send, att_recv,
 ):
@@ -543,21 +543,23 @@
     half = piece // 2
     length = piece * tp
     width = heads * LANES
-    here = {"sp": sp, "tp": me}
     partner = {"tp": y * 2 + 1 - core}
     opposite = {"tp": (1 - y) * 2 + core}
     beside = {"sp": z * 2 + 1 - x}
 
-    sources = (
-        tokens_in, norm_in, rotary_in, lam_in, w_key, w_value, w_query, w_rq, w_fwd, w_bwd, w_rv,
-        leak_in, decay_in, rec_gain_in, att_gain_in, out_rec_in, out_att_in,
+    small = (
+        (rotary_in, rotary), (lam_in, lam), (leak_in, leak), (decay_in, decay),
+        (rec_gain_in, rec_gain), (att_gain_in, att_gain),
     )
-    targets = (
-        tokens, gain, rotary, lam, *(weights.at[i] for i in range(7)),
-        leak, decay, rec_gain, att_gain, w_out_rec, w_out_att,
+    inputs = (w_key, w_value, w_query, w_rq, w_fwd, w_bwd, w_rv)
+    moves = (
+        [(tokens_in, tokens), (norm_in, gain)]
+        + [(a, weights.at[i]) for i, a in enumerate(inputs)]
+        + list(small) + [(out_rec_in, w_out_rec), (out_att_in, w_out_att)]
     )
-    fetches = [pltpu.make_async_copy(a, b, in_sem.at[i]) for i, (a, b) in enumerate(zip(sources, targets))]
-    for fetch in fetches:
+    fetches = [pltpu.make_async_copy(a, b, in_sem.at[i]) for i, (a, b) in enumerate(moves)]
+    f_rotary, f_lam, f_leak, f_decay, f_rec_gain, f_att_gain = fetches[9:15]
+    for fetch in fetches[:2] + fetches[9:11]:
         fetch.start()
 
     barrier = pltpu.get_barrier_semaphore()
@@ -573,151 +575,184 @@
             src_ref=source, dst_ref=target, send_sem=send, recv_sem=recv, device_id=to
         )
 
-    fetches[2].wait()
-    lane = lax.broadcasted_iota(jnp.int32, (piece, LANES), 1)
-    low_half = lax.rem(lane, AK) < AK // 2
-    for t in range(tp):
-        first = 2 * piece + sp * tp + t
-        cos_base = rotary[pl.ds(first, 1), :]
-        sin_base = rotary[pl.ds(first + ranks * tp, 1), :]
-        cos_row, sin_row = rotary[:piece, :], rotary[piece : 2 * piece, :]
-        cosine[t * piece : (t + 1) * piece, :] = cos_base * cos_row - sin_base * sin_row
-        turned = sin_base * cos_row + cos_base * sin_row
-        sine[t * piece : (t + 1) * piece, :] = jnp.where(low_half, -turned, turned)
-
-    def rows_of_piece(t, begin, count):
-        return held.at[pl.ds(pl.multiple_of(t * piece + begin, half), count)]
-
-    def across(part):
-        rows = rows_of_piece(me, part * half, half)
+    def held_at(owner, part, side):
+        return owner * 2 * piece + part * piece + side * half
+
+    def held_rows(owner, part, side):
+        return held.at[pl.ds(pl.multiple_of(held_at(owner, part, side), half), half)]
+
+    def across(part, owner):
+        rows = held_rows(owner, part, core)
         return remote(rows, rows, across_send.at[part], across_recv.at[part], opposite)
 
-    def from_across(part):
-        rows = rows_of_piece((1 - y) * 2 + core, part * half, half)
-        return remote(rows, rows, across_send.at[part], across_recv.at[part], opposite)
-
-    def to_core(t, slot, begin, count):
-        rows = rows_of_piece(t, begin, count)
+    def to_core(owner, part, side, slot):
+        rows = held_rows(owner, part, side)
         return remote(rows, rows, core_send.at[slot], core_recv.at[slot], partner)
 
     fetches[0].wait()
     fetches[1].wait()
+    for fetch in fetches[2:9] + fetches[11:15]:
+        fetch.start()
     for part in range(2):
         rows = tokens[part * half : (part + 1) * half, :].astype(F32)
-        held[pl.ds(pl.multiple_of(me * piece + part * half, half), half), :] = rms_scale(rows, gain[...]).astype(BF16)
+        at = pl.ds(pl.multiple_of(held_at(y, part, core), half), half)
+        held[at, :] = rms_scale(rows, gain[...]).astype(BF16)
         if part == 0:
             pl.semaphore_wait(barrier, planes * tp)
-        across(part).start()
-    to_core(me, 0, 0, piece).start()
-    fetches[3].wait()
+        across(part, y).start()
+        to_core(y, part, core, part).start()
+    f_lam.wait()
     for i in range(heads):
         lam_own[i] = jnp.broadcast_to(lam[:, i : i + 1], (8, LANES))
     lam_copy = remote(lam_own, lam_pair, lam_send, lam_recv, partner)
     lam_copy.start()
 
-    def rotated(wide, at):
-        turned = jnp.where(
-            jnp.concatenate([low_half] * 2, axis=0),
-            pltpu.roll(wide, LANES - AK // 2, 1), pltpu.roll(wide, AK // 2, 1),
-        )
-        return wide * cosine[at, :] + turned * sine[at, :]
-
-    def phase_rows(phase):
-        owner = y if phase == 0 else 1 - y
-        return pl.ds(pl.multiple_of(owner * 2 * piece, 2 * piece), 2 * piece)
-
-    def project(phase, index):
-        return jnp.dot(held[phase_rows(phase), :], weights[index], preferred_element_type=F32)
-
-    def qkv_target(i, c):
-        return core * heads + i, c
-
-    def qkv_copy(phase, i, c):
+    f_rotary.wait()
+    lane = lax.broadcasted_iota(jnp.int32, (piece, LANES), 1)
+    low_half = lax.rem(lane, AK) < AK // 2
+    for t in range(tp):
+        begin = 2 * piece + sp * tp + t
+        cos_base = rotary[pl.ds(begin, 1), :]
+        sin_base = rotary[pl.ds(begin + ranks * tp, 1), :]
+        cos_row, sin_row = rotary[:piece, :], rotary[piece : 2 * piece, :]
+        turned = sin_base * cos_row + cos_base * sin_row
+        cos_here = cos_base * cos_row - sin_base * sin_row
+        sin_here = jnp.where(low_half, -turned, turned)
+        for part in range(2):
+            to = held_at(t // 2, part, t % 2)
+            cosine[to : to + half, :] = cos_here[part * half : (part + 1) * half]
+            sine[to : to + half, :] = sin_here[part * half : (part + 1) * half]
+
+    def rotated(wide, cos_at, sin_at):
+        rows = wide.shape[0]
+        low = jnp.concatenate([low_half] * (rows // piece), axis=0)
+        turned = jnp.where(low, pltpu.roll(wide, LANES - AK // 2, 1), pltpu.roll(wide, AK // 2, 1))
+        return wide * cos_at + turned * sin_at
+
+    def owner_of(phase):
+        return y if phase < 2 else 1 - y
+
+    def plane_copy(phase, i, kind):
         return remote(
-            stage.at[phase, i, c], land.at[0, phase, z], qkv_send.at[phase, i, c], qkv_recv.at[phase, z],
+            stage_kv.at[phase, i, kind], kv.at[kind, 0, phase, z], kv_send.at[phase, i, kind], kv_recv.at[phase, z],
+            {"sp": (core * heads + i) * 2 + x, "tp": y * 2 + kind},
+        )
+
+    def query_rows(phase, plane):
+        return query.at[phase, pl.ds(pl.multiple_of(plane * half, half), half)]
+
+    def query_copy(phase, i, c):
+        return remote(
+            stage_q.at[phase, i, c], query_rows(phase, z), q_send.at[phase, i, c], q_recv.at[phase, z],
             {"sp": (core * heads + i) * 2 + x, "tp": y * 2 + c},
         )
 
-    def qkv_is_own(i, c):
+    def is_own(i, c):
         return jnp.logical_and(core * heads + i == z, core == c)
 
-    def attention_inputs(phase):
-        at = phase_rows(phase)
-        if phase == 0:
-            fetches[4].wait()
-        keys = project(phase, 0).astype(BF16).astype(F32)
-        if phase == 0:
-            fetches[5].wait()
-        values = project(phase, 1).astype(BF16).astype(F32)
-        if phase == 0:
-            fetches[6].wait()
-        queries = project(phase, 2).astype(BF16).astype(F32)
+    def project(at, index):
+        return jnp.dot(held[at, :], weights[index], preferred_element_type=F32)
+
+    def attention_inputs(phases):
+        count = len(phases) * piece
+        owner = owner_of(phases[0])
+        at = pl.ds(pl.multiple_of(held_at(owner, phases[0] % 2, 0), piece), count)
+        cos_at, sin_at = cosine[at, :], sine[at, :]
+        if phases[0] == 0:
+            fetches[2].wait()
+        keys = project(at, 0).astype(BF16).astype(F32)
+        if phases[0] == 0:
+            fetches[3].wait()
+        values = project(at, 1).astype(BF16).astype(F32)
         for i in range(heads):
             span = slice(i * LANES, (i + 1) * LANES)
-            key = rotated(keys[:, span], at).astype(BF16)
             value = values[:, span].T.astype(BF16)
-            query = (rotated(queries[:, span], at) * AK ** (-0.5)).astype(BF16)
-            for c in range(2):
-                part = slice(c * piece, (c + 1) * piece)
-                stage[phase, i, c, :piece, :] = key[part]
-                stage[phase, i, c, piece : 2 * piece, :] = value[:, part]
-                stage[phase, i, c, 2 * piece :, :] = query[part]
+            key = rotated(keys[:, span], cos_at, sin_at).astype(BF16)
+            for n, phase in enumerate(phases):
+                part = slice(n * piece, (n + 1) * piece)
+                stage_kv[phase, i, 0] = value[:, part]
+                stage_kv[phase, i, 1] = key[part]
+        for phase in phases:
+            send_each(phase, plane_copy, kv_recv, lambda i, c: (stage_kv.at[phase, i, c], kv.at[c, 0, phase, z]))
+        if phases[0] == 0:
+            fetches[4].wait()
+        queries = project(at, 2).astype(BF16).astype(F32)
+        for i in range(heads):
+            span = slice(i * LANES, (i + 1) * LANES)
+            turned = (rotated(queries[:, span], cos_at, sin_at) * AK ** (-0.5)).astype(BF16)
+            for n, phase in enumerate(phases):
+                for c in range(2):
+                    stage_q[phase, i, c] = turned[n * piece + c * half : n * piece + (c + 1) * half]
+        for phase in phases:
+            send_each(phase, query_copy, q_recv, lambda i, c: (stage_q.at[phase, i, c], query_rows(phase, z)))
+
+    def send_each(phase, copy, recv, local):
         for i in range(heads):
             for c in range(2):
-                own = qkv_is_own(i, c)
+                own = is_own(i, c)
 
                 @pl.when(own)
                 def _():
-                    pltpu.make_async_copy(
-                        stage.at[phase, i, c], land.at[0, phase, z], qkv_recv.at[phase, z]
-                    ).start()
+                    source, target = local(i, c)
+                    pltpu.make_async_copy(source, target, recv.at[phase, z]).start()
 
                 @pl.when(jnp.logical_not(own))
                 def _():
-                    qkv_copy(phase, i, c).start()
-
-    def recurrence_inputs(phase):
+                    copy(phase, i, c).start()
+
+    def recurrence_inputs(owner, wait):
+        at = pl.ds(pl.multiple_of(held_at(owner, 0, 0), 2 * piece), 2 * piece)
         for i in range(4):
-            if phase == 0:
-                fetches[7 + i].wait()
-            recp[i, phase_rows(phase), :] = project(phase, 3 + i).astype(BF16)
+            if wait:
+                fetches[5 + i].wait()
+            recp[i, at, :] = project(at, 3 + i).astype(BF16)
 
     def plane_at(k):
-        return (z, z + 1 - 2 * lax.rem(z, 2), lax.rem(z + 2, 4), planes - 1 - z)[k] if planes == 4 else lax.rem(z + k, planes)
-
-    def kv_of(origin, phase, plane):
-        return land.at[origin, phase, plane, : 2 * piece]
+        return (z, z + 1 - 2 * lax.rem(z, 2), lax.rem(z + 2, planes), planes - 1 - z)[k]
+
+    def mine_of(origin, phase, plane):
+        return kv.at[core, origin, phase, plane]
 
     def to_side(phase, plane):
         return remote(
-            kv_of(0, phase, plane), kv_of(2, phase, plane),
+            mine_of(0, phase, plane), mine_of(1, phase, plane),
             side_send.at[phase, plane], side_recv.at[phase, plane], beside,
         )
 
     def to_near(origin, phase, plane):
+        block = mine_of(origin, phase, plane)
         return remote(
-            kv_of(origin, phase, plane), kv_of(origin + 1, phase, plane),
-            near_send.at[origin // 2, phase, plane], near_recv.at[origin // 2, phase, plane], partner,
+            block, block, near_send.at[origin, phase, plane], near_recv.at[origin, phase, plane], partner
+        )
+
+    def from_near(origin, phase, plane):
+        block = kv.at[1 - core, origin, phase, plane]
+        return remote(
+            block, block, near_send.at[origin, phase, plane], near_recv.at[origin, phase, plane], partner
         )
 
     def relay_plane(phase, k):
         plane = plane_at(k)
-        remote(
-            land.at[0, phase, plane], land.at[0, phase, plane],
-            qkv_send.at[phase, 0, 0], qkv_recv.at[phase, plane], partner,
-        ).wait_recv()
+        block = mine_of(0, phase, plane)
+        remote(block, block, near_send.at[0, phase, plane], kv_recv.at[phase, plane], partner).wait_recv()
         to_side(phase, plane).start()
         to_near(0, phase, plane).start()
 
     def relay_side(phase, k):
         plane = plane_at(k)
-        to_side(phase, plane).wait_recv()
-        to_near(2, phase, plane).start()
+        block = mine_of(1, phase, plane)
+        remote(block, block, side_send.at[phase, plane], side_recv.at[phase, plane], beside).wait_recv()
+        to_near(1, phase, plane).start()
 
     def settle(phase):
         for k in range(planes):
-            for origin in (0, 2):
-                to_near(origin, phase, plane_at(k)).wait_recv()
+            for origin in range(2):
+                from_near(origin, phase, plane_at(k)).wait_recv()
+
+    def settle_queries(phase):
+        for k in range(planes):
+            rows = query_rows(phase, plane_at(k))
+            remote(rows, rows, q_send.at[phase, 0, 0], q_recv.at[phase, plane_at(k)], partner).wait_recv()
 
     row_at = lax.broadcasted_iota(jnp.int32, (BLOCK, 3 * BLOCK), 0)
     col_at = lax.rem(lax.broadcasted_iota(jnp.int32, (BLOCK, 3 * BLOCK), 1), BLOCK)
@@ -732,13 +767,17 @@
 
     def within_block(b):
         at = pl.ds(pl.multiple_of(b * BLOCK, BLOCK), BLOCK)
-        queries = jax.nn.silu(recp[0, at, :].astype(F32))
-        values = recp[3, at, :]
+        t = lax.div(b, 2)
+        stored = held_at(lax.div(t, 2), lax.rem(b, 2), lax.rem(t, 2))
+        held_block = pl.ds(pl.multiple_of(stored, BLOCK), BLOCK)
+        queries = jax.nn.silu(recp[0, held_block, :].astype(F32))
+        values = recp[3, held_block, :]
         scores, tails = [], []
         for d in range(2):
-            keys = leak[d : d + 1, :] * jax.nn.sigmoid(-recp[1 + d, at, :].astype(F32))
+            keys = leak[d : d + 1, :] * jax.nn.sigmoid(-recp[1 + d, held_block, :].astype(F32))
             added = jnp.concatenate(
-                [jnp.broadcast_to(decay[d, at, h : h + 1], (BLOCK, LANES)) for h in range(heads)], axis=1
+                [jnp.broadcast_to(decay_rows[at, d * heads + h : d * heads + h + 1], (BLOCK, LANES)) for h in range(heads)],
+                axis=1,
             )
             logs = jnp.log1p(-keys) + added
             coarse = logs.astype(BF16)
@@ -765,8 +804,7 @@
                 values[:, spans[h]], jnp.concatenate([tails[0][:, spans[h]], tails[1][:, spans[h]]], axis=1)
             )
 
-    def within_phase(phase):
-        owner = y if phase == 0 else 1 - y
+    def within_rows(owner):
         count = blocks // 2
 
         def some(j, carry):
@@ -884,162 +922,188 @@
     sub = 2 * piece
     ones = jnp.ones((PAD, sub), BF16)
     low_map = lane < AK
-    sub_count = 4 * planes * piece // sub
-
-    def key_block(phase, u, part):
-        block = 2 * u + part
-        return block // planes, phase, block % planes
-
-    def attend_step(phase, made, made_score, made_top, used, used_score):
+    chunk_blocks = 2 * planes
+    buffers = ((score_a, top_a), (score_b, top_b))
+
+    def attend_step(made, made_buffer, used, used_buffer):
         if made is not None:
-            q_phase, tile = made
-            query = land[0, q_phase, tile, 2 * piece :, :]
-            none = jnp.zeros_like(query)
-            both = jnp.concatenate([jnp.where(low_map, query, none), jnp.where(low_map, none, query)], axis=0)
+            q_phase, tile, made_phase = made
+            rows = query[q_phase, tile * piece : (tile + 1) * piece, :]
+            none = jnp.zeros_like(rows)
+            both = jnp.concatenate([jnp.where(low_map, rows, none), jnp.where(low_map, none, rows)], axis=0)
             top = None
         if used is not None:
-            q_phase_used, tile_used, used_top = used
-            slot = q_phase_used * planes + tile_used
+            slot, used_phase = used[0] * 2 + used[1], used[2]
+            used_score, used_top = used_buffer
             before = peak[slot][0:1]
             now = jnp.maximum(before, jnp.max(used_top[...], axis=0, keepdims=True))
             mixed = acc[slot] * jnp.exp(before - now)
-        for u in range(sub_count):
-            at = slice(u * sub, (u + 1) * sub)
+        for u in range(0, chunk_blocks, 2):
+            at = slice(u * piece, (u + 2) * piece)
+            where = [((u + n) // planes, (u + n) % planes) for n in range(2)]
             if made is not None:
-                keys = jnp.concatenate(
-                    [land[(*key_block(phase, u, part), slice(0, piece))] for part in range(2)], axis=0
-                )
+                keys = jnp.concatenate([kv[1, o, made_phase, p] for o, p in where], axis=0)
                 scores = dot_t(keys, both)
-                made_score[at, :] = scores
+                made_buffer[0][at, :] = scores
                 high = jnp.max(scores.reshape(sub // 8, 8, 2 * piece), axis=0)
                 top = high if top is None else jnp.maximum(top, high)
             if used is not None:
                 expo = jnp.exp(used_score[at, :] - now).astype(BF16)
-                values = jnp.concatenate(
-                    [land[(*key_block(phase, u, part), slice(piece, 2 * piece))] for part in range(2)], axis=1
-                )
+                values = jnp.concatenate([kv[0, o, used_phase, p] for o, p in where], axis=1)
                 values = jnp.concatenate([values, ones], axis=0)
                 mixed = mixed + jnp.dot(values, expo, preferred_element_type=F32)
         if used is not None:
             acc[slot] = mixed
             peak[slot] = jnp.broadcast_to(now, (8, 2 * piece))
         if made is not None:
-            made_top[...] = top
-
-    def attend(q_phase, phase, after):
-        attend_step(phase, (q_phase, 0), score_a, top_a, None, None)
-        buffers = ((score_a, top_a), (score_b, top_b))
-        for tile in range(1, planes + 1):
-            used_score, used_top = buffers[(tile - 1) % 2]
-            made_score, made_top = buffers[tile % 2]
-            made = (q_phase, tile) if tile < planes else None
-            attend_step(phase, made, made_score, made_top, (q_phase, tile - 1, used_top), used_score)
-            after(tile - 1)
-
-    def att_target(q_phase, tile):
-        owner = y if q_phase == 0 else 1 - y
-        return owner, {"sp": tile * 2 + x, "tp": owner * 2 + core}
-
-    def att_copy(q_phase, tile):
-        owner, to = att_target(q_phase, tile)
+            made_buffer[1][...] = top
+
+    def att_copy(q_phase, plane):
+        owner, part = owner_of(q_phase), q_phase % 2
         return remote(
-            att_stage.at[q_phase, tile], att_all.at[y * planes + z],
-            att_send.at[q_phase, tile], att_recv.at[y * planes + z], to,
+            att_stage.at[q_phase, plane], att_all.at[y * planes + z, part * half : (part + 1) * half],
+            att_send.at[q_phase, plane], att_recv.at[y * planes + z, part],
+            {"sp": plane * 2 + x, "tp": owner * 2 + core},
         )
 
     def finish(q_phase, tile):
-        whole = acc[q_phase * planes + tile]
+        whole = acc[q_phase * 2 + tile]
         ratio = whole[:LANES] / whole[LANES : LANES + 1]
         weight = jnp.where(core == lax.div(z, heads), lam_own[lax.rem(z, heads)], lam_pair[lax.rem(z, heads)])[0:1]
         values = ratio[:, :piece] - weight * ratio[:, piece:]
         scale = lax.rsqrt(jnp.mean(values * values, axis=0, keepdims=True) + EPS)
-        att_stage[q_phase, tile] = ((values * scale).T * att_gain[...]).astype(BF16)
-        if q_phase == 0:
-            own = tile == z
-
-            @pl.when(own)
-            def _():
-                pltpu.make_async_copy(
-                    att_stage.at[q_phase, tile], att_all.at[y * planes + z], att_recv.at[y * planes + z]
-                ).start()
-
-            @pl.when(jnp.logical_not(own))
-            def _():
-                att_copy(q_phase, tile).start()
-        else:
-            att_copy(q_phase, tile).start()
-
-    def att_arrival(index):
-        return remote(att_all.at[index], att_all.at[index], att_send.at[0, 0], att_recv.at[index], partner)
-
-    def nothing(tile):
-        pass
+        rows = ((values * scale).T * att_gain[...]).astype(BF16)
+        part = q_phase % 2
+        for n in range(2):
+            plane = 2 * tile + n
+            att_stage[q_phase, plane] = rows[n * half : (n + 1) * half]
+            if q_phase < 2:
+
+                @pl.when(plane == z)
+                def _():
+                    pltpu.make_async_copy(
+                        att_stage.at[q_phase, plane],
+                        att_all.at[y * planes + z, part * half : (part + 1) * half],
+                        att_recv.at[y * planes + z, part],
+                    ).start()
+
+                @pl.when(plane != z)
+                def _():
+                    att_copy(q_phase, plane).start()
+            else:
+                att_copy(q_phase, plane).start()
+
+    def att_arrival(index, part):
+        rows = att_all.at[index, part * half : (part + 1) * half]
+        return remote(rows, rows, att_send.at[0, 0], att_recv.at[index, part], partner)
 
     columns = min(512, out.shape[1])
 
-    to_core(y * 2 + 1 - core, 0, 0, piece).wait_recv()
-    attention_inputs(0)
-    recurrence_inputs(0)
-    for i in range(11, 15):
-        fetches[i].wait()
+    def rec_total():
+        for fetch in fetches[15:17]:
+            fetch.wait()
+        for dt in range(tp):
+            rec_arrival(dt).wait_recv()
+        rec_rows = jnp.concatenate([rec_all[t] for t in range(tp)], axis=1)
+        for n in range(0, out.shape[1], columns):
+            total[:, n : n + columns] = jnp.dot(rec_rows, w_out_rec[:, n : n + columns], preferred_element_type=F32)
+
+    def both_tiles(q_phase, key_phase):
+        return [(q_phase, tile, key_phase) for tile in range(2)]
+
+    def plan():
+        units, before = [], {}
+
+        def at_next(*actions):
+            before.setdefault(len(units), []).extend(actions)
+
+        def call(f, *args):
+            return functools.partial(f, *args)
+
+        at_next(call(settle, 0), call(settle_queries, 0))
+        units += both_tiles(0, 0)
+        at_next(*(call(relay_side, 1, k) for k in range(4)))
+        at_next(call(settle_queries, 1))
+        units += both_tiles(1, 0)
+        at_next(call(settle, 1))
+        units += both_tiles(0, 1)
+        at_next(pair_states, call(relay_plane, 2, 0), call(relay_plane, 2, 1))
+        units += both_tiles(1, 1)
+        at_next(call(relay_plane, 2, 2), call(relay_plane, 2, 3), call(settle_queries, 2))
+        units += [(2, 0, 0)]
+        at_next(*(call(relay_side, 2, k) for k in range(2)))
+        units += [(2, 1, 0)]
+        at_next(plane_states, call(relay_plane, 3, 0))
+        units += [(2, 0, 1)]
+        at_next(*(call(relay_side, 2, k) for k in range(2, 4)))
+        at_next(call(relay_plane, 3, 1))
+        units += [(2, 1, 1)]
+        at_next(call(settle, 2))
+        units += [(0, 0, 2)]
+        at_next(call(relay_plane, 3, 2))
+        units += [(0, 1, 2)]
+        at_next(call(relay_plane, 3, 3))
+        units += [(1, 0, 2)]
+        at_next(call(relay_side, 3, 0), call(relay_side, 3, 1))
+        units += [(1, 1, 2)]
+        at_next(call(relay_side, 3, 2))
+        units += both_tiles(2, 2)
+        at_next(call(relay_side, 3, 3), second_pass, call(settle_queries, 3))
+        units += both_tiles(3, 0) + both_tiles(3, 1) + both_tiles(3, 2)
+        at_next(call(settle, 3))
+        units += both_tiles(0, 3)
+        at_next(rec_total)
+        units += both_tiles(1, 3) + both_tiles(2, 3) + both_tiles(3, 3)
+        return units, before
+
+    for part in range(2):
+        to_core(y, part, 1 - core, part).wait_recv()
+    attention_inputs((0, 1))
+    for fetch in fetches[15:17]:
+        fetch.start()
+    recurrence_inputs(y, True)
+    for fetch in (f_leak, f_decay, f_rec_gain, f_att_gain):
+        fetch.wait()
+    by_row = jnp.concatenate([decay[d] for d in range(2)] + [jnp.zeros((LANES - 2 * heads, length), F32)], axis=0)
+    decay_rows[...] = by_row.T
     relay_plane(0, 0)
-    within_phase(0)
     relay_plane(0, 1)
-    for part in range(2):
-        from_across(part).wait_recv()
-        to_core((1 - y) * 2 + core, 1 + part, part * half, half).start()
-    relay_side(0, 0)
-    for part in range(2):
-        to_core((1 - y) * 2 + 1 - core, 1 + part, part * half, half).wait_recv()
-    attention_inputs(1)
+    relay_plane(1, 0)
+    within_rows(y)
+    across(0, 1 - y).wait_recv()
+    to_core(1 - y, 0, core, 2).start()
     relay_plane(0, 2)
     relay_plane(0, 3)
-    relay_side(0, 1)
-    recurrence_inputs(1)
-    within_phase(1)
+    to_core(1 - y, 0, 1 - core, 2).wait_recv()
+    attention_inputs((2,))
+    for k in range(4):
+        relay_side(0, k)
+    relay_plane(1, 1)
+    across(1, 1 - y).wait_recv()
+    to_core(1 - y, 1, core, 3).start()
+    relay_plane(1, 2)
+    to_core(1 - y, 1, 1 - core, 3).wait_recv()
+    attention_inputs((3,))
+    relay_plane(1, 3)
+    recurrence_inputs(1 - y, False)
+    within_rows(1 - y)
     local_states()
     pair_copy.start()
-    relay_plane(1, 0)
-    relay_side(0, 2)
-    relay_side(0, 3)
-    settle(0)
     lam_copy.wait_recv()
 
-    def while_early(tile):
-        if tile == 0:
-            pair_states()
-            relay_plane(1, 1)
-        if tile == 1:
-            relay_plane(1, 2)
-            relay_side(1, 0)
-        if tile == 2:
-            relay_plane(1, 3)
-
-    attend(0, 0, while_early)
-
-    def while_later(tile):
-        if tile == 0:
-            relay_side(1, 1)
-            plane_states()
-        if tile == 1:
-            relay_side(1, 2)
-        if tile == 2:
-            relay_side(1, 3)
-
-    attend(1, 0, while_later)
-    second_pass()
-    settle(1)
-    attend(0, 1, functools.partial(finish, 0))
-    fetches[15].wait()
-    fetches[16].wait()
-    for dt in range(tp):
-        rec_arrival(dt).wait_recv()
-    rec_rows = jnp.concatenate([rec_all[t] for t in range(tp)], axis=1)
-    for n in range(0, out.shape[1], columns):
-        total[:, n : n + columns] = jnp.dot(rec_rows, w_out_rec[:, n : n + columns], preferred_element_type=F32)
-    attend(1, 1, functools.partial(finish, 1))
-    for index in range(2 * planes):
-        att_arrival(index).wait_recv()
+    units, before = plan()
+    for n in range(len(units) + 1):
+        for action in before.get(n, ()):
+            action()
+        made = units[n] if n < len(units) else None
+        used = units[n - 1] if n else None
+        attend_step(made, buffers[n % 2], used, buffers[(n + 1) % 2])
+        if used is not None and used[2] == 3:
+            finish(used[0], used[1])
+
+    for part in range(2):
+        for index in range(2 * planes):
+            att_arrival(index, part).wait_recv()
     att_rows = jnp.concatenate([att_all[i] for i in range(2 * planes)], axis=1)
     for n in range(0, out.shape[1], columns):
         out[:, n : n + columns] = (
@@ -1048,35 +1112,38 @@
         ).astype(BF16)
 
     for part in range(2):
-        across(part).wait_send()
-        to_core((1 - y) * 2 + core, 1 + part, part * half, half).wait_send()
-    to_core(me, 0, 0, piece).wait_send()
+        across(part, y).wait_send()
+        to_core(y, part, core, part).wait_send()
+        to_core(1 - y, part, core, 2 + part).wait_send()
     lam_copy.wait_send()
-    for phase in range(2):
+    for phase in range(4):
         for i in range(heads):
             for c in range(2):
 
-                @pl.when(jnp.logical_not(qkv_is_own(i, c)))
+                @pl.when(jnp.logical_not(is_own(i, c)))
                 def _():
-                    qkv_copy(phase, i, c).wait_send()
+                    plane_copy(phase, i, c).wait_send()
+                    query_copy(phase, i, c).wait_send()
 
         for k in range(planes):
             to_side(phase, plane_at(k)).wait_send()
             to_near(0, phase, plane_at(k)).wait_send()
-            to_near(2, phase, plane_at(k)).wait_send()
+            to_near(1, phase, plane_at(k)).wait_send()
     pair_copy.wait_send()
     next_copy.wait_send()
     for dz in range(1, planes):
         to_plane(lax.rem(z + dz, planes)).wait_send()
     for dt in range(1, tp):
         rec_copy(dt).wait_send()
-    for tile in range(planes):
-
-        @pl.when(tile != z)
-        def _():
-            att_copy(0, tile).wait_send()
-
-        att_copy(1, tile).wait_send()
+    for plane in range(planes):
+        for phase in range(4):
+            if phase < 2:
+
+                @pl.when(plane != z)
+                def _():
+                    att_copy(phase, plane).wait_send()
+            else:
+                att_copy(phase, plane).wait_send()
 
 
 def rotary_table(piece, pieces):
@@ -1103,7 +1170,7 @@
     length = piece * tp
     width = heads * LANES
     blocks = length // BLOCK
-    keys = 4 * planes * piece
+    keys = 2 * planes * piece
     anywhere = pl.BlockSpec(memory_space=pl.ANY)
     dma = pltpu.SemaphoreType.DMA
     vmem = pltpu.VMEM
@@ -1118,7 +1185,8 @@
             vmem((1, model), F32),
             vmem((7, model, width), BF16),
             vmem((2, width), F32),
-            vmem((2, length, heads), F32),
+            vmem((2, heads, length), F32),
+            vmem((length, LANES), F32),
             vmem((1, LANES), F32),
             vmem((1, heads), F32),
             vmem((1, LANES), F32),
@@ -1130,8 +1198,10 @@
             vmem((length, LANES), F32),
             vmem((heads, 8, LANES), F32),
             vmem((heads, 8, LANES), F32),
-            vmem((2, heads, 2, 3 * piece, LANES), BF16),
-            vmem((4, 2, planes, 3 * piece, LANES), BF16),
+            vmem((4, heads, 2, piece, LANES), BF16),
+            vmem((4, heads, 2, piece // 2, LANES), BF16),
+            vmem((2, 2, 4, planes, piece, LANES), BF16),
+            vmem((4, planes * piece // 2, LANES), BF16),
             vmem((4, length, width), BF16),
             vmem((heads, length, 2 * LANES), BF16),
             vmem((blocks, 2, 8, width), F32),
@@ -1155,14 +1225,14 @@
             vmem((8, 2 * piece), F32),
             vmem((2 * planes, LANES + PAD, 2 * piece), F32),
             vmem((2 * planes, 8, 2 * piece), F32),
-            vmem((2, planes, piece, LANES), BF16),
+            vmem((4, planes, piece // 2, LANES), BF16),
             vmem((2 * planes, piece, LANES), BF16),
             vmem((piece, model), F32),
-            dma((17,)), dma((2,)), dma((2,)), dma((3,)), dma((3,)), dma, dma,
-            dma((2, heads, 2)), dma((2, planes)), dma((2, planes)), dma((2, planes)),
-            dma((2, 2, planes)), dma((2, 2, planes)),
+            dma((17,)), dma((2,)), dma((2,)), dma((4,)), dma((4,)), dma, dma,
+            dma((4, heads, 2)), dma((4, planes)), dma((4, heads, 2)), dma((4, planes)),
+            dma((4, planes)), dma((4, planes)), dma((2, 4, planes)), dma((2, 4, planes)),
             dma, dma, dma((planes,)), dma((planes,)), dma, dma,
-            dma((tp,)), dma((tp,)), dma((2, planes)), dma((2 * planes,)),
+            dma((tp,)), dma((tp,)), dma((4, planes)), dma((2 * planes, 2)),
         ],
         compiler_params=pltpu.CompilerParams(
             collective_id=2, has_side_effects=True, vmem_limit_bytes=60 * 1024 * 1024
@@ -1170,7 +1240,7 @@
         cost_estimate=pl.CostEstimate(flops=10**10, bytes_accessed=10**7, transcendentals=10**7),
     )(
         tokens, norm_gain.reshape(1, -1), att_key, att_value, att_query, rec_query, fwd_gate, bwd_gate, rec_value,
-        gate_leak, log_decay, rec_gain.reshape(1, LANES), lambdas.reshape(1, heads), att_gain.reshape(1, LANES),
+        gate_leak, log_decay.transpose(0, 2, 1), rec_gain.reshape(1, LANES), lambdas.reshape(1, heads), att_gain.reshape(1, LANES),
         out_rec, out_att, table,
     )
 

time: 57.2 us -> 61 us (1.066)
  Pallas kernels: 53.4 us -> 59 us
  local copies, waits for them, and re-layouts: 3.6 us -> 1.88 us
    pallas_call x1, Pallas kernels: 53.4 us -> 59 us  [on_device(): pl.pallas_call(functools.partial(fused_kernel, ranks, tp, heads, planes),...]
    unnamed x2 -> x1, local copies, waits for them, and re-layouts: 3.6 us -> 1.88 us
where the time goes in v2:
time: 61 us; the launch traced here: 60.8 us
  Pallas kernels  59 us (97%)
  local copies, waits for them, and re-layouts  1.88 us (3%)
    pallas_call x1, Pallas kernels, on_device(): pl.pallas_call(functools.partial(fused_kernel, ranks, tp, heads, planes),...  59 us
    unnamed x1, local copies, waits for them, and re-layouts  1.88 us

profile of v2, /device:TPU:0, one launch (start us, length us, event | category | flops | bytes accessed | tf_op | source)
XLA Modules:
  0.0 60.8 jit_solution(9154134810896921687)
XLA Ops:
  0.0 59.0 %shard_map.163 = bf16[128,2048]{1,0:T(8,128)(2,1)} custom-call(bf16[128,2048]{1,0:T(8,128)(2,1)} %tokens_in.1, f32[1,2048]{1,0:T(1,128)} %bitcast.5, bf16[2048,256]{1,0:T(8,128)(2,1)} %w_key.1, bf16[2048,256]{1,0:T(8,128)(2,1)} %w_value.1, bf16[2048,256]{1,0:T(8,128)(2,1)} %w_query.1, bf16[2048,256]{1,0:T(8,128)(2,1)} %w_rq.1, bf16[2048,256]{1,0:T(8,128)(2,1)} %w_fwd.1, ...), custom_call_target="tpu_custom_call" | custom-call | flops 10000000000 | bytes 10000000 | tf_op jit(solution)/shard_map/pallas_call | solution.py:1178
  59.0 1.9 %copy.19 = bf16[128,2048]{1,0:T(8,128)(2,1)} copy(bf16[128,2048]{1,0:T(8,128)(2,1)} %shard_map.163) | data formatting | bytes 1048576

commit v3 on v2

--- a/solution.py
+++ b/solution.py
@@ -524,11 +524,11 @@
     tokens_in, norm_in, w_key, w_value, w_query, w_rq, w_fwd, w_bwd, w_rv, leak_in, decay_in, rec_gain_in,
     lam_in, att_gain_in, out_rec_in, out_att_in, rotary_in,
     out,
-    tokens, gain, weights, leak, decay, decay_rows, rec_gain, lam, att_gain, w_out_rec, w_out_att, rotary,
+    tokens, gain, weights, leak, decay, decay_rows, rec_gain, lam, att_gain, w_out, rotary,
     held, cosine, sine, lam_own, lam_pair, stage_kv, stage_q, kv, query, recp, cum_reads, facts, adds, rec_sum,
     state, fade, pair_out, pair_in, plane_out, plane_in, plane_sum, next_out, next_in, before_block,
     rec_stage, rec_all, score_a, score_b, top_a, top_b, acc, peak, att_stage, att_all, total,
-    in_sem, across_send, across_recv, core_send, core_recv, lam_send, lam_recv,
+    up, down, in_sem, across_send, across_recv, core_send, core_recv, lam_send, lam_recv,
     kv_send, kv_recv, q_send, q_recv, side_send, side_recv, near_send, near_recv,
     pair_send, pair_recv, plane_send, plane_recv, next_send, next_recv,
     rec_send, rec_recv, att_send, att_recv,
@@ -555,20 +555,58 @@
     moves = (
         [(tokens_in, tokens), (norm_in, gain)]
         + [(a, weights.at[i]) for i, a in enumerate(inputs)]
-        + list(small) + [(out_rec_in, w_out_rec), (out_att_in, w_out_att)]
+        + list(small) + [(out_rec_in, w_out.at[0]), (out_att_in, w_out.at[1])]
     )
-    fetches = [pltpu.make_async_copy(a, b, in_sem.at[i]) for i, (a, b) in enumerate(moves)]
+    slots = (0, 1, 2, 3, 4, 5, 5, 5, 5, 6, 7, 8, 9, 10, 11, 12, 12)
+    fetches = [pltpu.make_async_copy(a, b, in_sem.at[i]) for i, (a, b) in zip(slots, moves)]
     f_rotary, f_lam, f_leak, f_decay, f_rec_gain, f_att_gain = fetches[9:15]
     for fetch in fetches[:2] + fetches[9:11]:
         fetch.start()
 
     barrier = pltpu.get_barrier_semaphore()
-    for dz in range(planes):
-        for dt in range(tp):
-            if dz or dt:
-                to = {"sp": lax.rem(z + dz, planes) * 2 + x, "tp": lax.rem(me + dt, tp)}
-                pl.semaphore_signal(barrier, inc=1, device_id=to)
-    pl.semaphore_signal(barrier, inc=1, device_id=beside)
+    above = {"sp": sp + 2}
+    below = {"sp": sp - 2}
+    for to in (partner, opposite, {"tp": (1 - y) * 2 + 1 - core}, beside):
+        pl.semaphore_signal(barrier, inc=1, device_id=to)
+
+    @pl.when(z > 0)
+    def _():
+        pl.semaphore_signal(barrier, inc=1, device_id=below)
+
+    @pl.when(z < planes - 1)
+    def _():
+        pl.semaphore_signal(barrier, inc=1, device_id=above)
+
+    neighbours = 4 + lax.div(z + planes - 2, planes - 1) + lax.div(2 * planes - 3 - z, planes - 1)
+
+    def chains():
+        def pass_up():
+            @pl.when(z > 0)
+            def _():
+                pl.semaphore_wait(up, 1)
+
+            @pl.when(z < planes - 1)
+            def _():
+                pl.semaphore_signal(up, inc=1, device_id=above)
+
+        def pass_down():
+            @pl.when(z < planes - 1)
+            def _():
+                pl.semaphore_wait(down, 1)
+
+            @pl.when(z > 0)
+            def _():
+                pl.semaphore_signal(down, inc=1, device_id=below)
+
+        @pl.when(2 * z < planes)
+        def _():
+            pass_up()
+            pass_down()
+
+        @pl.when(2 * z >= planes)
+        def _():
+            pass_down()
+            pass_up()
 
     def remote(source, target, send, recv, to):
         return pltpu.make_async_remote_copy(
@@ -583,11 +621,11 @@
 
     def across(part, owner):
         rows = held_rows(owner, part, core)
-        return remote(rows, rows, across_send.at[part], across_recv.at[part], opposite)
+        return remote(rows, rows, across_send, across_recv.at[part], opposite)
 
     def to_core(owner, part, side, slot):
         rows = held_rows(owner, part, side)
-        return remote(rows, rows, core_send.at[slot], core_recv.at[slot], partner)
+        return remote(rows, rows, core_send, core_recv.at[slot], partner)
 
     fetches[0].wait()
     fetches[1].wait()
@@ -598,7 +636,7 @@
         at = pl.ds(pl.multiple_of(held_at(y, part, core), half), half)
         held[at, :] = rms_scale(rows, gain[...]).astype(BF16)
         if part == 0:
-            pl.semaphore_wait(barrier, planes * tp)
+            pl.semaphore_wait(barrier, neighbours)
         across(part, y).start()
         to_core(y, part, core, part).start()
     f_lam.wait()
@@ -634,7 +672,7 @@
 
     def plane_copy(phase, i, kind):
         return remote(
-            stage_kv.at[phase, i, kind], kv.at[kind, 0, phase, z], kv_send.at[phase, i, kind], kv_recv.at[phase, z],
+            stage_kv.at[phase, i, kind], kv.at[kind, 0, phase, z], kv_send, kv_recv.at[phase, z],
             {"sp": (core * heads + i) * 2 + x, "tp": y * 2 + kind},
         )
 
@@ -643,7 +681,7 @@
 
     def query_copy(phase, i, c):
         return remote(
-            stage_q.at[phase, i, c], query_rows(phase, z), q_send.at[phase, i, c], q_recv.at[phase, z],
+            stage_q.at[phase, i, c], query_rows(phase, z), q_send, q_recv.at[phase],
             {"sp": (core * heads + i) * 2 + x, "tp": y * 2 + c},
         )
 
@@ -672,8 +710,10 @@
                 part = slice(n * piece, (n + 1) * piece)
                 stage_kv[phase, i, 0] = value[:, part]
                 stage_kv[phase, i, 1] = key[part]
+        if phases[0] == 0:
+            chains()
         for phase in phases:
-            send_each(phase, plane_copy, kv_recv, lambda i, c: (stage_kv.at[phase, i, c], kv.at[c, 0, phase, z]))
+            send_each(phase, plane_copy, kv_recv.at[phase, z], lambda i, c: (stage_kv.at[phase, i, c], kv.at[c, 0, phase, z]))
         if phases[0] == 0:
             fetches[4].wait()
         queries = project(at, 2).astype(BF16).astype(F32)
@@ -684,7 +724,7 @@
                 for c in range(2):
                     stage_q[phase, i, c] = turned[n * piece + c * half : n * piece + (c + 1) * half]
         for phase in phases:
-            send_each(phase, query_copy, q_recv, lambda i, c: (stage_q.at[phase, i, c], query_rows(phase, z)))
+            send_each(phase, query_copy, q_recv.at[phase], lambda i, c: (stage_q.at[phase, i, c], query_rows(phase, z)))
 
     def send_each(phase, copy, recv, local):
         for i in range(heads):
@@ -694,7 +734,7 @@
                 @pl.when(own)
                 def _():
                     source, target = local(i, c)
-                    pltpu.make_async_copy(source, target, recv.at[phase, z]).start()
+                    pltpu.make_async_copy(source, target, recv).start()
 
                 @pl.when(jnp.logical_not(own))
                 def _():
@@ -702,9 +742,9 @@
 
     def recurrence_inputs(owner, wait):
         at = pl.ds(pl.multiple_of(held_at(owner, 0, 0), 2 * piece), 2 * piece)
+        if wait:
+            pltpu.make_async_copy(weights.at[3:7], weights.at[3:7], in_sem.at[5]).wait()
         for i in range(4):
-            if wait:
-                fetches[5 + i].wait()
             recp[i, at, :] = project(at, 3 + i).astype(BF16)
 
     def plane_at(k):
@@ -716,43 +756,35 @@
     def to_side(phase, plane):
         return remote(
             mine_of(0, phase, plane), mine_of(1, phase, plane),
-            side_send.at[phase, plane], side_recv.at[phase, plane], beside,
+            side_send, side_recv.at[phase, plane], beside,
         )
 
     def to_near(origin, phase, plane):
         block = mine_of(origin, phase, plane)
         return remote(
-            block, block, near_send.at[origin, phase, plane], near_recv.at[origin, phase, plane], partner
-        )
-
-    def from_near(origin, phase, plane):
-        block = kv.at[1 - core, origin, phase, plane]
-        return remote(
-            block, block, near_send.at[origin, phase, plane], near_recv.at[origin, phase, plane], partner
+            block, block, near_send, near_recv.at[phase], partner
         )
 
     def relay_plane(phase, k):
         plane = plane_at(k)
         block = mine_of(0, phase, plane)
-        remote(block, block, near_send.at[0, phase, plane], kv_recv.at[phase, plane], partner).wait_recv()
+        remote(block, block, near_send, kv_recv.at[phase, plane], partner).wait_recv()
         to_side(phase, plane).start()
         to_near(0, phase, plane).start()
 
     def relay_side(phase, k):
         plane = plane_at(k)
         block = mine_of(1, phase, plane)
-        remote(block, block, side_send.at[phase, plane], side_recv.at[phase, plane], beside).wait_recv()
+        remote(block, block, side_send, side_recv.at[phase, plane], beside).wait_recv()
         to_near(1, phase, plane).start()
 
     def settle(phase):
-        for k in range(planes):
-            for origin in range(2):
-                from_near(origin, phase, plane_at(k)).wait_recv()
+        blocks_in = kv.at[1 - core, :, phase]
+        remote(blocks_in, blocks_in, near_send, near_recv.at[phase], partner).wait_recv()
 
     def settle_queries(phase):
-        for k in range(planes):
-            rows = query_rows(phase, plane_at(k))
-            remote(rows, rows, q_send.at[phase, 0, 0], q_recv.at[phase, plane_at(k)], partner).wait_recv()
+        rows = query.at[phase]
+        remote(rows, rows, q_send, q_recv.at[phase], partner).wait_recv()
 
     row_at = lax.broadcasted_iota(jnp.int32, (BLOCK, 3 * BLOCK), 0)
     col_at = lax.rem(lax.broadcasted_iota(jnp.int32, (BLOCK, 3 * BLOCK), 1), BLOCK)
@@ -860,24 +892,22 @@
     def to_plane(target):
         return remote(
             plane_out.at[jnp.where(target > z, 0, 1)], plane_in.at[z],
-            plane_send.at[target], plane_recv.at[z], {"sp": target * 2 + x},
-        )
-
-    def from_plane(source):
-        return remote(
-            plane_out.at[0], plane_in.at[source],
-            plane_send.at[source], plane_recv.at[source], {"sp": source * 2 + x},
-        )
+            plane_send, plane_recv, {"sp": target * 2 + x},
+        )
+
+    def other_planes():
+        blocks_in = plane_in.at[: planes - 1]
+        return remote(blocks_in, blocks_in, plane_send, plane_recv, partner)
 
     next_copy = remote(next_out, next_in, next_send, next_recv, beside)
 
     def plane_states():
+        other_planes().wait_recv()
         plane_sum[...] = jnp.zeros_like(plane_sum)
 
         def fold(d):
             def one(step, carry):
                 plane = step if d == 0 else planes - 1 - step
-                from_plane(plane).wait_recv()
                 moved, factor = unpack(plane_in.at[plane])
                 plane_sum[d] = plane_sum[d] * factor + moved
                 return carry
@@ -910,12 +940,8 @@
         t = lax.rem(me + dt, tp)
         source = rec_stage.at[pl.ds(pl.multiple_of(t * piece, piece), piece)]
         if dt == 0:
-            return pltpu.make_async_copy(source, rec_all.at[me], rec_recv.at[me])
-        return remote(source, rec_all.at[me], rec_send.at[dt], rec_recv.at[me], {"tp": t})
-
-    def rec_arrival(dt):
-        t = lax.rem(me + dt, tp)
-        return remote(rec_all.at[t], rec_all.at[t], rec_send.at[dt], rec_recv.at[t], {"tp": t})
+            return pltpu.make_async_copy(source, rec_all.at[me], rec_recv)
+        return remote(source, rec_all.at[me], rec_send, rec_recv, {"tp": t})
 
     acc[...] = jnp.zeros_like(acc)
     peak[...] = jnp.full_like(peak, -jnp.inf)
@@ -961,8 +987,8 @@
     def att_copy(q_phase, plane):
         owner, part = owner_of(q_phase), q_phase % 2
         return remote(
-            att_stage.at[q_phase, plane], att_all.at[y * planes + z, part * half : (part + 1) * half],
-            att_send.at[q_phase, plane], att_recv.at[y * planes + z, part],
+            att_stage.at[q_phase * planes + plane], att_all.at[y * planes + z, part * half : (part + 1) * half],
+            att_send, att_recv,
             {"sp": plane * 2 + x, "tp": owner * 2 + core},
         )
 
@@ -976,15 +1002,15 @@
         part = q_phase % 2
         for n in range(2):
             plane = 2 * tile + n
-            att_stage[q_phase, plane] = rows[n * half : (n + 1) * half]
+            att_stage[q_phase * planes + plane] = rows[n * half : (n + 1) * half]
             if q_phase < 2:
 
                 @pl.when(plane == z)
                 def _():
                     pltpu.make_async_copy(
-                        att_stage.at[q_phase, plane],
+                        att_stage.at[q_phase * planes + plane],
                         att_all.at[y * planes + z, part * half : (part + 1) * half],
-                        att_recv.at[y * planes + z, part],
+                        att_recv,
                     ).start()
 
                 @pl.when(plane != z)
@@ -993,20 +1019,24 @@
             else:
                 att_copy(q_phase, plane).start()
 
-    def att_arrival(index, part):
-        rows = att_all.at[index, part * half : (part + 1) * half]
-        return remote(rows, rows, att_send.at[0, 0], att_recv.at[index, part], partner)
-
     columns = min(512, out.shape[1])
 
     def rec_total():
-        for fetch in fetches[15:17]:
-            fetch.wait()
-        for dt in range(tp):
-            rec_arrival(dt).wait_recv()
+        pltpu.make_async_copy(w_out, w_out, in_sem.at[12]).wait()
+        remote(rec_all, rec_all, rec_send, rec_recv, partner).wait_recv()
         rec_rows = jnp.concatenate([rec_all[t] for t in range(tp)], axis=1)
         for n in range(0, out.shape[1], columns):
-            total[:, n : n + columns] = jnp.dot(rec_rows, w_out_rec[:, n : n + columns], preferred_element_type=F32)
+            total[:, n : n + columns] = jnp.dot(rec_rows, w_out[0, :, n : n + columns], preferred_element_type=F32)
+
+    def run_units(units, before):
+        for n in range(len(units) + 1):
+            for action in before.get(n, ()):
+                action()
+            made = units[n] if n < len(units) else None
+            used = units[n - 1] if n else None
+            attend_step(made, buffers[n % 2], used, buffers[(n + 1) % 2])
+            if used is not None and used[2] == 3:
+                finish(used[0], used[1])
 
     def both_tiles(q_phase, key_phase):
         return [(q_phase, tile, key_phase) for tile in range(2)]
@@ -1020,35 +1050,22 @@
         def call(f, *args):
             return functools.partial(f, *args)
 
-        at_next(call(settle, 0), call(settle_queries, 0))
-        units += both_tiles(0, 0)
-        at_next(*(call(relay_side, 1, k) for k in range(4)))
-        at_next(call(settle_queries, 1))
+        units += both_tiles(0, 1)
+        at_next(pair_states, *(call(relay_side, 2, k) for k in range(2)))
         units += both_tiles(1, 0)
-        at_next(call(settle, 1))
-        units += both_tiles(0, 1)
-        at_next(pair_states, call(relay_plane, 2, 0), call(relay_plane, 2, 1))
+        at_next(*(call(relay_side, 2, k) for k in range(2, 4)))
         units += both_tiles(1, 1)
-        at_next(call(relay_plane, 2, 2), call(relay_plane, 2, 3), call(settle_queries, 2))
-        units += [(2, 0, 0)]
-        at_next(*(call(relay_side, 2, k) for k in range(2)))
-        units += [(2, 1, 0)]
-        at_next(plane_states, call(relay_plane, 3, 0))
-        units += [(2, 0, 1)]
-        at_next(*(call(relay_side, 2, k) for k in range(2, 4)))
-        at_next(call(relay_plane, 3, 1))
-        units += [(2, 1, 1)]
-        at_next(call(settle, 2))
-        units += [(0, 0, 2)]
-        at_next(call(relay_plane, 3, 2))
-        units += [(0, 1, 2)]
-        at_next(call(relay_plane, 3, 3))
-        units += [(1, 0, 2)]
+        at_next(call(settle_queries, 2), plane_states, *(call(relay_plane, 3, k) for k in range(3)))
+        units += both_tiles(2, 0)
+        at_next(call(relay_plane, 3, 3), call(settle, 2))
+        units += both_tiles(2, 1)
         at_next(call(relay_side, 3, 0), call(relay_side, 3, 1))
-        units += [(1, 1, 2)]
-        at_next(call(relay_side, 3, 2))
+        units += both_tiles(0, 2)
+        at_next(call(relay_side, 3, 2), call(relay_side, 3, 3))
+        units += both_tiles(1, 2)
+        at_next(second_pass)
         units += both_tiles(2, 2)
-        at_next(call(relay_side, 3, 3), second_pass, call(settle_queries, 3))
+        at_next(call(settle_queries, 3))
         units += both_tiles(3, 0) + both_tiles(3, 1) + both_tiles(3, 2)
         at_next(call(settle, 3))
         units += both_tiles(0, 3)
@@ -1067,9 +1084,8 @@
     by_row = jnp.concatenate([decay[d] for d in range(2)] + [jnp.zeros((LANES - 2 * heads, length), F32)], axis=0)
     decay_rows[...] = by_row.T
     relay_plane(0, 0)
+    within_rows(y)
     relay_plane(0, 1)
-    relay_plane(1, 0)
-    within_rows(y)
     across(0, 1 - y).wait_recv()
     to_core(1 - y, 0, core, 2).start()
     relay_plane(0, 2)
@@ -1078,72 +1094,64 @@
     attention_inputs((2,))
     for k in range(4):
         relay_side(0, k)
+    relay_plane(1, 0)
     relay_plane(1, 1)
+    lam_copy.wait_recv()
+    settle(0)
+    settle_queries(0)
+    run_units(both_tiles(0, 0), {})
     across(1, 1 - y).wait_recv()
     to_core(1 - y, 1, core, 3).start()
     relay_plane(1, 2)
+    relay_plane(1, 3)
     to_core(1 - y, 1, 1 - core, 3).wait_recv()
     attention_inputs((3,))
-    relay_plane(1, 3)
+    for k in range(4):
+        relay_side(1, k)
     recurrence_inputs(1 - y, False)
+    relay_plane(2, 0)
     within_rows(1 - y)
     local_states()
     pair_copy.start()
-    lam_copy.wait_recv()
-
-    units, before = plan()
-    for n in range(len(units) + 1):
-        for action in before.get(n, ()):
-            action()
-        made = units[n] if n < len(units) else None
-        used = units[n - 1] if n else None
-        attend_step(made, buffers[n % 2], used, buffers[(n + 1) % 2])
-        if used is not None and used[2] == 3:
-            finish(used[0], used[1])
-
-    for part in range(2):
-        for index in range(2 * planes):
-            att_arrival(index, part).wait_recv()
+    for k in range(1, 4):
+        relay_plane(2, k)
+    settle(1)
+    settle_queries(1)
+    run_units(*plan())
+
+    remote(att_all, att_all, att_send, att_recv, partner).wait_recv()
     att_rows = jnp.concatenate([att_all[i] for i in range(2 * planes)], axis=1)
     for n in range(0, out.shape[1], columns):
         out[:, n : n + columns] = (
             total[:, n : n + columns]
-            + jnp.dot(att_rows, w_out_att[:, n : n + columns], preferred_element_type=F32)
+            + jnp.dot(att_rows, w_out[1, :, n : n + columns], preferred_element_type=F32)
         ).astype(BF16)
 
-    for part in range(2):
-        across(part, y).wait_send()
-        to_core(y, part, core, part).wait_send()
-        to_core(1 - y, part, core, 2 + part).wait_send()
+    def sent(ref, sem, recv):
+        remote(ref, ref, sem, recv, partner).wait_send()
+
+    sent(held.at[:piece], across_send, core_recv.at[0])
+    sent(held.at[: 2 * piece], core_send, core_recv.at[0])
     lam_copy.wait_send()
-    for phase in range(4):
-        for i in range(heads):
-            for c in range(2):
-
-                @pl.when(jnp.logical_not(is_own(i, c)))
-                def _():
-                    plane_copy(phase, i, c).wait_send()
-                    query_copy(phase, i, c).wait_send()
-
-        for k in range(planes):
-            to_side(phase, plane_at(k)).wait_send()
-            to_near(0, phase, plane_at(k)).wait_send()
-            to_near(1, phase, plane_at(k)).wait_send()
+    is_local = core == lax.div(z, heads)
+
+    @pl.when(is_local)
+    def _():
+        sent(stage_kv.at[:3], kv_send, near_recv.at[0])
+        sent(stage_q.at[:3], q_send, near_recv.at[0])
+
+    @pl.when(jnp.logical_not(is_local))
+    def _():
+        sent(stage_kv, kv_send, near_recv.at[0])
+        sent(stage_q, q_send, near_recv.at[0])
+
+    sent(kv.at[0, 0], side_send, near_recv.at[0])
+    sent(kv.at[0], near_send, near_recv.at[0])
     pair_copy.wait_send()
     next_copy.wait_send()
-    for dz in range(1, planes):
-        to_plane(lax.rem(z + dz, planes)).wait_send()
-    for dt in range(1, tp):
-        rec_copy(dt).wait_send()
-    for plane in range(planes):
-        for phase in range(4):
-            if phase < 2:
-
-                @pl.when(plane != z)
-                def _():
-                    att_copy(phase, plane).wait_send()
-            else:
-                att_copy(phase, plane).wait_send()
+    sent(plane_in.at[: planes - 1], plane_send, plane_recv)
+    sent(rec_all.at[: tp - 1], rec_send, rec_recv)
+    sent(att_stage.at[: 4 * planes - 2], att_send, att_recv)
 
 
 def rotary_table(piece, pieces):
@@ -1190,8 +1198,7 @@
             vmem((1, LANES), F32),
             vmem((1, heads), F32),
             vmem((1, LANES), F32),
-            vmem(out_rec.shape, BF16),
-            vmem(out_att.shape, BF16),
+            vmem((2, *out_rec.shape), BF16),
             vmem(table.shape, F32),
             vmem((length, model), BF16),
             vmem((length, LANES), F32),
@@ -1225,14 +1232,15 @@
             vmem((8, 2 * piece), F32),
             vmem((2 * planes, LANES + PAD, 2 * piece), F32),
             vmem((2 * planes, 8, 2 * piece), F32),
-            vmem((4, planes, piece // 2, LANES), BF16),
+            vmem((4 * planes, piece // 2, LANES), BF16),
             vmem((2 * planes, piece, LANES), BF16),
             vmem((piece, model), F32),
-            dma((17,)), dma((2,)), dma((2,)), dma((4,)), dma((4,)), dma, dma,
-            dma((4, heads, 2)), dma((4, planes)), dma((4, heads, 2)), dma((4, planes)),
-            dma((4, planes)), dma((4, planes)), dma((2, 4, planes)), dma((2, 4, planes)),
-            dma, dma, dma((planes,)), dma((planes,)), dma, dma,
-            dma((tp,)), dma((tp,)), dma((4, planes)), dma((2 * planes, 2)),
+            pltpu.SemaphoreType.REGULAR, pltpu.SemaphoreType.REGULAR,
+            dma((13,)), dma, dma((2,)), dma, dma((4,)), dma, dma,
+            dma, dma((4, planes)), dma, dma((4,)),
+            dma, dma((4, planes)), dma, dma((4,)),
+            dma, dma, dma, dma, dma, dma,
+            dma, dma, dma, dma,
         ],
         compiler_params=pltpu.CompilerParams(
             collective_id=2, has_side_effects=True, vmem_limit_bytes=60 * 1024 * 1024

time: 61 us -> 61.4 us (level)
  no operation moved by 1% of the time
where the time goes in v3:
time: 61.4 us; the launch traced here: 61.2 us
  Pallas kernels  59.3 us (97%)
  local copies, waits for them, and re-layouts  1.88 us (3%)
    pallas_call x1, Pallas kernels, on_device(): pl.pallas_call(functools.partial(fused_kernel, ranks, tp, heads, planes),...  59.3 us
    unnamed x1, local copies, waits for them, and re-layouts  1.88 us

profile of v3, /device:TPU:0, one launch (start us, length us, event | category | flops | bytes accessed | tf_op | source)
XLA Modules:
  0.0 61.2 jit_solution(17589579250309594494)
XLA Ops:
  0.0 59.3 %shard_map.163 = bf16[128,2048]{1,0:T(8,128)(2,1)} custom-call(bf16[128,2048]{1,0:T(8,128)(2,1)} %tokens_in.1, f32[1,2048]{1,0:T(1,128)} %bitcast.5, bf16[2048,256]{1,0:T(8,128)(2,1)} %w_key.1, bf16[2048,256]{1,0:T(8,128)(2,1)} %w_value.1, bf16[2048,256]{1,0:T(8,128)(2,1)} %w_query.1, bf16[2048,256]{1,0:T(8,128)(2,1)} %w_rq.1, bf16[2048,256]{1,0:T(8,128)(2,1)} %w_fwd.1, ...), custom_call_target="tpu_custom_call" | custom-call | flops 10000000000 | bytes 10000000 | tf_op jit(solution)/shard_map/pallas_call | solution.py:1186
  59.3 1.9 %copy.19 = bf16[128,2048]{1,0:T(8,128)(2,1)} copy(bf16[128,2048]{1,0:T(8,128)(2,1)} %shard_map.163) | data formatting | bytes 1048576

commit v4 on v3

--- a/solution.py
+++ b/solution.py
@@ -948,34 +948,35 @@
     sub = 2 * piece
     ones = jnp.ones((PAD, sub), BF16)
     low_map = lane < AK
-    chunk_blocks = 2 * planes
     buffers = ((score_a, top_a), (score_b, top_b))
 
     def attend_step(made, made_buffer, used, used_buffer):
         if made is not None:
-            q_phase, tile, made_phase = made
+            q_phase, tile, made_phases = made
+            chunk = made_phases
             rows = query[q_phase, tile * piece : (tile + 1) * piece, :]
             none = jnp.zeros_like(rows)
             both = jnp.concatenate([jnp.where(low_map, rows, none), jnp.where(low_map, none, rows)], axis=0)
             top = None
         if used is not None:
-            slot, used_phase = used[0] * 2 + used[1], used[2]
+            slot, chunk = used[0] * 2 + used[1], used[2]
             used_score, used_top = used_buffer
             before = peak[slot][0:1]
             now = jnp.maximum(before, jnp.max(used_top[...], axis=0, keepdims=True))
             mixed = acc[slot] * jnp.exp(before - now)
-        for u in range(0, chunk_blocks, 2):
+        for u in range(0, 2 * planes * len(chunk), 2):
             at = slice(u * piece, (u + 2) * piece)
-            where = [((u + n) // planes, (u + n) % planes) for n in range(2)]
+            turn, pair = u // (2 * planes), u % (2 * planes)
+            where = [((pair + n) // planes, (pair + n) % planes) for n in range(2)]
             if made is not None:
-                keys = jnp.concatenate([kv[1, o, made_phase, p] for o, p in where], axis=0)
+                keys = jnp.concatenate([kv[1, o, made_phases[turn], p] for o, p in where], axis=0)
                 scores = dot_t(keys, both)
                 made_buffer[0][at, :] = scores
                 high = jnp.max(scores.reshape(sub // 8, 8, 2 * piece), axis=0)
                 top = high if top is None else jnp.maximum(top, high)
             if used is not None:
                 expo = jnp.exp(used_score[at, :] - now).astype(BF16)
-                values = jnp.concatenate([kv[0, o, used_phase, p] for o, p in where], axis=1)
+                values = jnp.concatenate([kv[0, o, used[2][turn], p] for o, p in where], axis=1)
                 values = jnp.concatenate([values, ones], axis=0)
                 mixed = mixed + jnp.dot(values, expo, preferred_element_type=F32)
         if used is not None:
@@ -1035,47 +1036,35 @@
             made = units[n] if n < len(units) else None
             used = units[n - 1] if n else None
             attend_step(made, buffers[n % 2], used, buffers[(n + 1) % 2])
-            if used is not None and used[2] == 3:
+            if used is not None and used[2][-1] == 3:
                 finish(used[0], used[1])
 
-    def both_tiles(q_phase, key_phase):
-        return [(q_phase, tile, key_phase) for tile in range(2)]
-
-    def plan():
-        units, before = [], {}
-
-        def at_next(*actions):
-            before.setdefault(len(units), []).extend(actions)
-
-        def call(f, *args):
-            return functools.partial(f, *args)
-
-        units += both_tiles(0, 1)
-        at_next(pair_states, *(call(relay_side, 2, k) for k in range(2)))
-        units += both_tiles(1, 0)
-        at_next(*(call(relay_side, 2, k) for k in range(2, 4)))
-        units += both_tiles(1, 1)
-        at_next(call(settle_queries, 2), plane_states, *(call(relay_plane, 3, k) for k in range(3)))
-        units += both_tiles(2, 0)
-        at_next(call(relay_plane, 3, 3), call(settle, 2))
-        units += both_tiles(2, 1)
-        at_next(call(relay_side, 3, 0), call(relay_side, 3, 1))
-        units += both_tiles(0, 2)
-        at_next(call(relay_side, 3, 2), call(relay_side, 3, 3))
-        units += both_tiles(1, 2)
-        at_next(second_pass)
-        units += both_tiles(2, 2)
-        at_next(call(settle_queries, 3))
-        units += both_tiles(3, 0) + both_tiles(3, 1) + both_tiles(3, 2)
-        at_next(call(settle, 3))
-        units += both_tiles(0, 3)
-        at_next(rec_total)
-        units += both_tiles(1, 3) + both_tiles(2, 3) + both_tiles(3, 3)
-        return units, before
+    def tiles_of(q_phases, chunk):
+        return [(q_phase, tile, chunk) for q_phase in q_phases for tile in range(2)]
+
+    def call(f, *args):
+        return functools.partial(f, *args)
+
+    def all_of(f, phase, ks):
+        return [call(f, phase, k) for k in ks]
+
+    near, far = (0, 1), (2, 3)
+    units = tiles_of(near, near) + tiles_of(far, near) + tiles_of(near, far) + tiles_of(far, far)
+    before = {
+        1: [call(relay_plane, 2, 0), call(relay_plane, 2, 1)],
+        2: [call(relay_plane, 2, 2), call(relay_plane, 2, 3), pair_states],
+        3: all_of(relay_side, 2, range(2)),
+        4: all_of(relay_plane, 3, range(4)) + [call(settle_queries, 2), call(settle_queries, 3)],
+        5: all_of(relay_side, 2, range(2, 4)) + [plane_states],
+        6: all_of(relay_side, 3, range(2)),
+        7: all_of(relay_side, 3, range(2, 4)),
+        8: [call(settle, 2), call(settle, 3)],
+        12: [second_pass],
+    }
 
     for part in range(2):
         to_core(y, part, 1 - core, part).wait_recv()
-    attention_inputs((0, 1))
+    attention_inputs(near)
     for fetch in fetches[15:17]:
         fetch.start()
     recurrence_inputs(y, True)
@@ -1084,40 +1073,38 @@
     by_row = jnp.concatenate([decay[d] for d in range(2)] + [jnp.zeros((LANES - 2 * heads, length), F32)], axis=0)
     decay_rows[...] = by_row.T
     relay_plane(0, 0)
+    relay_plane(1, 0)
     within_rows(y)
     relay_plane(0, 1)
     across(0, 1 - y).wait_recv()
     to_core(1 - y, 0, core, 2).start()
     relay_plane(0, 2)
     relay_plane(0, 3)
-    to_core(1 - y, 0, 1 - core, 2).wait_recv()
-    attention_inputs((2,))
-    for k in range(4):
-        relay_side(0, k)
-    relay_plane(1, 0)
-    relay_plane(1, 1)
-    lam_copy.wait_recv()
-    settle(0)
-    settle_queries(0)
-    run_units(both_tiles(0, 0), {})
+    relay_side(0, 0)
     across(1, 1 - y).wait_recv()
     to_core(1 - y, 1, core, 3).start()
+    relay_plane(1, 1)
+    for part in range(2):
+        to_core(1 - y, part, 1 - core, 2 + part).wait_recv()
+    attention_inputs(far)
     relay_plane(1, 2)
     relay_plane(1, 3)
-    to_core(1 - y, 1, 1 - core, 3).wait_recv()
-    attention_inputs((3,))
-    for k in range(4):
-        relay_side(1, k)
+    for k in range(1, 4):
+        relay_side(0, k)
     recurrence_inputs(1 - y, False)
-    relay_plane(2, 0)
+    relay_side(1, 0)
+    relay_side(1, 1)
     within_rows(1 - y)
     local_states()
     pair_copy.start()
-    for k in range(1, 4):
-        relay_plane(2, k)
-    settle(1)
-    settle_queries(1)
-    run_units(*plan())
+    relay_side(1, 2)
+    relay_side(1, 3)
+    lam_copy.wait_recv()
+    for phase in near:
+        settle(phase)
+        settle_queries(phase)
+    run_units(units, before)
+    rec_total()
 
     remote(att_all, att_all, att_send, att_recv, partner).wait_recv()
     att_rows = jnp.concatenate([att_all[i] for i in range(2 * planes)], axis=1)
@@ -1178,7 +1165,7 @@
     length = piece * tp
     width = heads * LANES
     blocks = length // BLOCK
-    keys = 2 * planes * piece
+    keys = 4 * planes * piece
     anywhere = pl.BlockSpec(memory_space=pl.ANY)
     dma = pltpu.SemaphoreType.DMA
     vmem = pltpu.VMEM

time: 61.4 us -> 53.6 us (0.87)
  Pallas kernels: 59.3 us -> 51.5 us
    pallas_call x1, Pallas kernels: 59.3 us -> 51.5 us  [on_device(): pl.pallas_call(functools.partial(fused_kernel, ranks, tp, heads, planes),...]
where the time goes in v4:
time: 53.6 us; the launch traced here: 53.4 us
  Pallas kernels  51.5 us (96%)
  local copies, waits for them, and re-layouts  1.88 us (4%)
    pallas_call x1, Pallas kernels, on_device(): pl.pallas_call(functools.partial(fused_kernel, ranks, tp, heads, planes),...  51.5 us
    unnamed x1, local copies, waits for them, and re-layouts  1.88 us

profile of v4, /device:TPU:0, one launch (start us, length us, event | category | flops | bytes accessed | tf_op | source)
XLA Modules:
  0.0 53.4 jit_solution(8557360715750671477)
XLA Ops:
  0.0 51.5 %shard_map.163 = bf16[128,2048]{1,0:T(8,128)(2,1)} custom-call(bf16[128,2048]{1,0:T(8,128)(2,1)} %tokens_in.1, f32[1,2048]{1,0:T(1,128)} %bitcast.5, bf16[2048,256]{1,0:T(8,128)(2,1)} %w_key.1, bf16[2048,256]{1,0:T(8,128)(2,1)} %w_value.1, bf16[2048,256]{1,0:T(8,128)(2,1)} %w_query.1, bf16[2048,256]{1,0:T(8,128)(2,1)} %w_rq.1, bf16[2048,256]{1,0:T(8,128)(2,1)} %w_fwd.1, ...), custom_call_target="tpu_custom_call" | custom-call | flops 10000000000 | bytes 10000000 | tf_op jit(solution)/shard_map/pallas_call | solution.py:1173
  51.5 1.9 %copy.19 = bf16[128,2048]{1,0:T(8,128)(2,1)} copy(bf16[128,2048]{1,0:T(8,128)(2,1)} %shard_map.163) | data formatting | bytes 1048576

commit v5 on v4

--- a/solution.py
+++ b/solution.py
@@ -579,34 +579,15 @@
 
     neighbours = 4 + lax.div(z + planes - 2, planes - 1) + lax.div(2 * planes - 3 - z, planes - 1)
 
-    def chains():
-        def pass_up():
-            @pl.when(z > 0)
+    def hop(turn):
+        for toward, signal, source in ((above, up, 0), (below, down, planes - 1)):
+
+            @pl.when(z == (turn if source == 0 else source - turn))
             def _():
-                pl.semaphore_wait(up, 1)
-
-            @pl.when(z < planes - 1)
-            def _():
-                pl.semaphore_signal(up, inc=1, device_id=above)
-
-        def pass_down():
-            @pl.when(z < planes - 1)
-            def _():
-                pl.semaphore_wait(down, 1)
-
-            @pl.when(z > 0)
-            def _():
-                pl.semaphore_signal(down, inc=1, device_id=below)
-
-        @pl.when(2 * z < planes)
-        def _():
-            pass_up()
-            pass_down()
-
-        @pl.when(2 * z >= planes)
-        def _():
-            pass_down()
-            pass_up()
+                if turn:
+                    pl.semaphore_wait(signal, 1)
+                if turn < planes - 1:
+                    pl.semaphore_signal(signal, inc=1, device_id=toward)
 
     def remote(source, target, send, recv, to):
         return pltpu.make_async_remote_copy(
@@ -637,6 +618,7 @@
         held[at, :] = rms_scale(rows, gain[...]).astype(BF16)
         if part == 0:
             pl.semaphore_wait(barrier, neighbours)
+            hop(0)
         across(part, y).start()
         to_core(y, part, core, part).start()
     f_lam.wait()
@@ -661,6 +643,8 @@
             cosine[to : to + half, :] = cos_here[part * half : (part + 1) * half]
             sine[to : to + half, :] = sin_here[part * half : (part + 1) * half]
 
+    hop(1)
+
     def rotated(wide, cos_at, sin_at):
         rows = wide.shape[0]
         low = jnp.concatenate([low_half] * (rows // piece), axis=0)
@@ -702,6 +686,8 @@
         if phases[0] == 0:
             fetches[3].wait()
         values = project(at, 1).astype(BF16).astype(F32)
+        if phases[0] == 0:
+            hop(2)
         for i in range(heads):
             span = slice(i * LANES, (i + 1) * LANES)
             value = values[:, span].T.astype(BF16)
@@ -711,7 +697,7 @@
                 stage_kv[phase, i, 0] = value[:, part]
                 stage_kv[phase, i, 1] = key[part]
         if phases[0] == 0:
-            chains()
+            hop(3)
         for phase in phases:
             send_each(phase, plane_copy, kv_recv.at[phase, z], lambda i, c: (stage_kv.at[phase, i, c], kv.at[c, 0, phase, z]))
         if phases[0] == 0:
@@ -762,7 +748,7 @@
     def to_near(origin, phase, plane):
         block = mine_of(origin, phase, plane)
         return remote(
-            block, block, near_send, near_recv.at[phase], partner
+            block, block, near_send, near_recv.at[phase, origin], partner
         )
 
     def relay_plane(phase, k):
@@ -778,9 +764,9 @@
         remote(block, block, side_send, side_recv.at[phase, plane], beside).wait_recv()
         to_near(1, phase, plane).start()
 
-    def settle(phase):
-        blocks_in = kv.at[1 - core, :, phase]
-        remote(blocks_in, blocks_in, near_send, near_recv.at[phase], partner).wait_recv()
+    def settle(phase, origin):
+        blocks_in = kv.at[1 - core, origin, phase]
+        remote(blocks_in, blocks_in, near_send, near_recv.at[phase, origin], partner).wait_recv()
 
     def settle_queries(phase):
         rows = query.at[phase]
@@ -836,7 +822,7 @@
                 values[:, spans[h]], jnp.concatenate([tails[0][:, spans[h]], tails[1][:, spans[h]]], axis=1)
             )
 
-    def within_rows(owner):
+    def within_rows(owner, turns):
         count = blocks // 2
 
         def some(j, carry):
@@ -844,7 +830,7 @@
             within_block(owner * count + 2 * j + 1)
             return carry
 
-        lax.fori_loop(0, count // 2, some, 0)
+        lax.fori_loop(turns[0], turns[-1] + 1, some, 0)
 
     def order(d):
         return range(blocks) if d == 0 else range(blocks - 1, -1, -1)
@@ -877,10 +863,22 @@
                 fade[d, h] = jnp.broadcast_to(factor, (8, LANES))
                 pack(pair_out.at[d, h], moved, factor)
 
-    pair_copy = remote(pair_out, pair_in, pair_send, pair_recv, beside)
+    def pair_copies():
+        return [
+            remote(pair_out.at[d, h], pair_in.at[d, h], pair_send, pair_recv, beside)
+            for d, h in ((0, 1 - x), (1, 1 - x), (x, x))
+        ]
+
+    def pair_done():
+        three = plane_in.at[:3]
+        return remote(three, three, pair_send, pair_recv, beside)
+
+    def send_pair():
+        for copy in pair_copies():
+            copy.start()
 
     def pair_states():
-        pair_copy.wait_recv()
+        pair_done().wait_recv()
         for d in range(2):
             mine, factor = state[d, x], fade[d, x][0:1]
             other, other_factor = unpack(pair_in.at[d, x])
@@ -924,7 +922,7 @@
         for h in range(heads):
             for d in range(2):
                 entering = jnp.where(x == h, plane_sum[d], next_in[d].astype(F32))
-                other, other_factor = unpack(pair_in.at[d, h])
+                other, other_factor = unpack(pair_in.at[d, jnp.where(x == d, x, h)])
                 running = jnp.where(x == d, entering, entering * other_factor + other)
                 for b in order(d):
                     before_block[b, h, :, half_of(d)] = running.astype(BF16)
@@ -952,31 +950,32 @@
 
     def attend_step(made, made_buffer, used, used_buffer):
         if made is not None:
-            q_phase, tile, made_phases = made
-            chunk = made_phases
+            q_phase, tile, chunk = made
+            made_blocks = [(o, f, p) for f, o in chunk for p in range(planes)]
             rows = query[q_phase, tile * piece : (tile + 1) * piece, :]
             none = jnp.zeros_like(rows)
             both = jnp.concatenate([jnp.where(low_map, rows, none), jnp.where(low_map, none, rows)], axis=0)
             top = None
         if used is not None:
-            slot, chunk = used[0] * 2 + used[1], used[2]
+            slot = used[0] * 2 + used[1]
+            used_blocks = [(o, f, p) for f, o in used[2] for p in range(planes)]
             used_score, used_top = used_buffer
             before = peak[slot][0:1]
             now = jnp.maximum(before, jnp.max(used_top[...], axis=0, keepdims=True))
             mixed = acc[slot] * jnp.exp(before - now)
-        for u in range(0, 2 * planes * len(chunk), 2):
-            at = slice(u * piece, (u + 2) * piece)
-            turn, pair = u // (2 * planes), u % (2 * planes)
-            where = [((pair + n) // planes, (pair + n) % planes) for n in range(2)]
-            if made is not None:
-                keys = jnp.concatenate([kv[1, o, made_phases[turn], p] for o, p in where], axis=0)
+        made_pairs = len(made_blocks) // 2 if made is not None else 0
+        used_pairs = len(used_blocks) // 2 if used is not None else 0
+        for u in range(max(made_pairs, used_pairs)):
+            at = slice(u * sub, (u + 1) * sub)
+            if u < made_pairs:
+                keys = jnp.concatenate([kv[(1, *block)] for block in made_blocks[2 * u : 2 * u + 2]], axis=0)
                 scores = dot_t(keys, both)
                 made_buffer[0][at, :] = scores
                 high = jnp.max(scores.reshape(sub // 8, 8, 2 * piece), axis=0)
                 top = high if top is None else jnp.maximum(top, high)
-            if used is not None:
+            if u < used_pairs:
                 expo = jnp.exp(used_score[at, :] - now).astype(BF16)
-                values = jnp.concatenate([kv[0, o, used[2][turn], p] for o, p in where], axis=1)
+                values = jnp.concatenate([kv[(0, *block)] for block in used_blocks[2 * u : 2 * u + 2]], axis=1)
                 values = jnp.concatenate([values, ones], axis=0)
                 mixed = mixed + jnp.dot(values, expo, preferred_element_type=F32)
         if used is not None:
@@ -1036,7 +1035,7 @@
             made = units[n] if n < len(units) else None
             used = units[n - 1] if n else None
             attend_step(made, buffers[n % 2], used, buffers[(n + 1) % 2])
-            if used is not None and used[2][-1] == 3:
+            if used is not None and used[2][-1] == (3, 1):
                 finish(used[0], used[1])
 
     def tiles_of(q_phases, chunk):
@@ -1049,18 +1048,23 @@
         return [call(f, phase, k) for k in ks]
 
     near, far = (0, 1), (2, 3)
-    units = tiles_of(near, near) + tiles_of(far, near) + tiles_of(near, far) + tiles_of(far, far)
+    near_keys = [(f, o) for f in near for o in range(2)]
+    far_keys = [(f, o) for f in far for o in range(2)]
+    every = near + far
+    units = tiles_of(every, near_keys) + tiles_of(every, far_keys)
     before = {
-        1: [call(relay_plane, 2, 0), call(relay_plane, 2, 1)],
-        2: [call(relay_plane, 2, 2), call(relay_plane, 2, 3), pair_states],
-        3: all_of(relay_side, 2, range(2)),
-        4: all_of(relay_plane, 3, range(4)) + [call(settle_queries, 2), call(settle_queries, 3)],
-        5: all_of(relay_side, 2, range(2, 4)) + [plane_states],
-        6: all_of(relay_side, 3, range(2)),
-        7: all_of(relay_side, 3, range(2, 4)),
-        8: [call(settle, 2), call(settle, 3)],
+        1: [call(relay_plane, 3, 0)],
+        2: [call(relay_plane, 3, 1)] + all_of(relay_side, 2, range(1)),
+        3: [call(relay_plane, 3, 2)] + all_of(relay_side, 2, range(1, 2)),
+        4: [call(settle_queries, 2), call(settle_queries, 3), call(relay_plane, 3, 3)],
+        5: all_of(relay_side, 2, range(2, 4)),
+        6: all_of(relay_side, 3, range(1)),
+        7: all_of(relay_side, 3, range(1, 3)),
+        8: all_of(relay_side, 3, range(3, 4)) + [call(settle, f, o) for f, o in far_keys],
+        9: [plane_states],
         12: [second_pass],
     }
+    before[4].append(pair_states)
 
     for part in range(2):
         to_core(y, part, 1 - core, part).wait_recv()
@@ -1074,34 +1078,41 @@
     decay_rows[...] = by_row.T
     relay_plane(0, 0)
     relay_plane(1, 0)
-    within_rows(y)
+    within_rows(y, (0, 1))
     relay_plane(0, 1)
     across(0, 1 - y).wait_recv()
     to_core(1 - y, 0, core, 2).start()
     relay_plane(0, 2)
+    to_core(1 - y, 0, 1 - core, 2).wait_recv()
+    attention_inputs((2,))
     relay_plane(0, 3)
     relay_side(0, 0)
+    relay_plane(1, 1)
     across(1, 1 - y).wait_recv()
     to_core(1 - y, 1, core, 3).start()
-    relay_plane(1, 1)
-    for part in range(2):
-        to_core(1 - y, part, 1 - core, 2 + part).wait_recv()
-    attention_inputs(far)
+    to_core(1 - y, 1, 1 - core, 3).wait_recv()
+    attention_inputs((3,))
     relay_plane(1, 2)
     relay_plane(1, 3)
     for k in range(1, 4):
         relay_side(0, k)
+    relay_plane(2, 0)
     recurrence_inputs(1 - y, False)
     relay_side(1, 0)
     relay_side(1, 1)
-    within_rows(1 - y)
-    local_states()
-    pair_copy.start()
+    relay_plane(2, 1)
+    within_rows(1 - y, (0,))
     relay_side(1, 2)
     relay_side(1, 3)
+    relay_plane(2, 2)
+    within_rows(1 - y, (1,))
+    relay_plane(2, 3)
+    local_states()
+    send_pair()
     lam_copy.wait_recv()
     for phase in near:
-        settle(phase)
+        for origin in range(2):
+            settle(phase, origin)
         settle_queries(phase)
     run_units(units, before)
     rec_total()
@@ -1124,17 +1135,17 @@
 
     @pl.when(is_local)
     def _():
-        sent(stage_kv.at[:3], kv_send, near_recv.at[0])
-        sent(stage_q.at[:3], q_send, near_recv.at[0])
+        sent(stage_kv.at[:3], kv_send, near_recv.at[0, 0])
+        sent(stage_q.at[:3], q_send, near_recv.at[0, 0])
 
     @pl.when(jnp.logical_not(is_local))
     def _():
-        sent(stage_kv, kv_send, near_recv.at[0])
-        sent(stage_q, q_send, near_recv.at[0])
-
-    sent(kv.at[0, 0], side_send, near_recv.at[0])
-    sent(kv.at[0], near_send, near_recv.at[0])
-    pair_copy.wait_send()
+        sent(stage_kv, kv_send, near_recv.at[0, 0])
+        sent(stage_q, q_send, near_recv.at[0, 0])
+
+    sent(kv.at[0, 0], side_send, near_recv.at[0, 0])
+    sent(kv.at[0], near_send, near_recv.at[0, 0])
+    pair_done().wait_send()
     next_copy.wait_send()
     sent(plane_in.at[: planes - 1], plane_send, plane_recv)
     sent(rec_all.at[: tp - 1], rec_send, rec_recv)
@@ -1225,7 +1236,7 @@
             pltpu.SemaphoreType.REGULAR, pltpu.SemaphoreType.REGULAR,
             dma((13,)), dma, dma((2,)), dma, dma((4,)), dma, dma,
             dma, dma((4, planes)), dma, dma((4,)),
-            dma, dma((4, planes)), dma, dma((4,)),
+            dma, dma((4, planes)), dma, dma((4, 2)),
             dma, dma, dma, dma, dma, dma,
             dma, dma, dma, dma,
         ],

time: 53.6 us -> 51.5 us (0.961)
  Pallas kernels: 51.5 us -> 49.5 us
    pallas_call x1, Pallas kernels: 51.5 us -> 49.5 us  [on_device(): pl.pallas_call(functools.partial(fused_kernel, ranks, tp, heads, planes),...]
where the time goes in v5:
time: 51.5 us; the launch traced here: 51.4 us
  Pallas kernels  49.5 us (96%)
  local copies, waits for them, and re-layouts  1.88 us (4%)
    pallas_call x1, Pallas kernels, on_device(): pl.pallas_call(functools.partial(fused_kernel, ranks, tp, heads, planes),...  49.5 us
    unnamed x1, local copies, waits for them, and re-layouts  1.88 us

profile of v5, /device:TPU:0, one launch (start us, length us, event | category | flops | bytes accessed | tf_op | source)
XLA Modules:
  0.0 51.4 jit_solution(2098456457177816961)
XLA Ops:
  0.0 49.5 %shard_map.163 = bf16[128,2048]{1,0:T(8,128)(2,1)} custom-call(bf16[128,2048]{1,0:T(8,128)(2,1)} %tokens_in.1, f32[1,2048]{1,0:T(1,128)} %bitcast.5, bf16[2048,256]{1,0:T(8,128)(2,1)} %w_key.1, bf16[2048,256]{1,0:T(8,128)(2,1)} %w_value.1, bf16[2048,256]{1,0:T(8,128)(2,1)} %w_query.1, bf16[2048,256]{1,0:T(8,128)(2,1)} %w_rq.1, bf16[2048,256]{1,0:T(8,128)(2,1)} %w_fwd.1, ...), custom_call_target="tpu_custom_call" | custom-call | flops 10000000000 | bytes 10000000 | tf_op jit(solution)/shard_map/pallas_call | solution.py:1184
  49.5 1.9 %copy.19 = bf16[128,2048]{1,0:T(8,128)(2,1)} copy(bf16[128,2048]{1,0:T(8,128)(2,1)} %shard_map.163) | data formatting | bytes 1048576

commit v6 on v5

--- a/solution.py
+++ b/solution.py
@@ -726,8 +726,8 @@
                 def _():
                     copy(phase, i, c).start()
 
-    def recurrence_inputs(owner, wait):
-        at = pl.ds(pl.multiple_of(held_at(owner, 0, 0), 2 * piece), 2 * piece)
+    def recurrence_inputs(owner, parts, wait):
+        at = pl.ds(pl.multiple_of(held_at(owner, parts[0], 0), piece), len(parts) * piece)
         if wait:
             pltpu.make_async_copy(weights.at[3:7], weights.at[3:7], in_sem.at[5]).wait()
         for i in range(4):
@@ -822,15 +822,13 @@
                 values[:, spans[h]], jnp.concatenate([tails[0][:, spans[h]], tails[1][:, spans[h]]], axis=1)
             )
 
-    def within_rows(owner, turns):
-        count = blocks // 2
-
-        def some(j, carry):
-            within_block(owner * count + 2 * j)
-            within_block(owner * count + 2 * j + 1)
+    def within_rows(owner, parts):
+        def some(part, carry):
+            within_block(owner * 4 + part)
+            within_block(owner * 4 + 2 + part)
             return carry
 
-        lax.fori_loop(turns[0], turns[-1] + 1, some, 0)
+        lax.fori_loop(parts[0], parts[-1] + 1, some, 0)
 
     def order(d):
         return range(blocks) if d == 0 else range(blocks - 1, -1, -1)
@@ -952,7 +950,7 @@
         if made is not None:
             q_phase, tile, chunk = made
             made_blocks = [(o, f, p) for f, o in chunk for p in range(planes)]
-            rows = query[q_phase, tile * piece : (tile + 1) * piece, :]
+            rows = query[q_phase, pl.ds(tile * piece if isinstance(tile, int) else pl.multiple_of(tile * piece, piece), piece), :]
             none = jnp.zeros_like(rows)
             both = jnp.concatenate([jnp.where(low_map, rows, none), jnp.where(low_map, none, rows)], axis=0)
             top = None
@@ -1051,7 +1049,10 @@
     near_keys = [(f, o) for f in near for o in range(2)]
     far_keys = [(f, o) for f in far for o in range(2)]
     every = near + far
-    units = tiles_of(every, near_keys) + tiles_of(every, far_keys)
+    units = tiles_of(every, near_keys)
+    side_tile = 1 - lax.div(2 * z, planes)
+    for tile in (side_tile, 1 - side_tile):
+        units += [(q_phase, tile, far_keys) for q_phase in every]
     before = {
         1: [call(relay_plane, 3, 0)],
         2: [call(relay_plane, 3, 1)] + all_of(relay_side, 2, range(1)),
@@ -1071,7 +1072,7 @@
     attention_inputs(near)
     for fetch in fetches[15:17]:
         fetch.start()
-    recurrence_inputs(y, True)
+    recurrence_inputs(y, (0, 1), True)
     for fetch in (f_leak, f_decay, f_rec_gain, f_att_gain):
         fetch.wait()
     by_row = jnp.concatenate([decay[d] for d in range(2)] + [jnp.zeros((LANES - 2 * heads, length), F32)], axis=0)
@@ -1088,27 +1089,28 @@
     relay_plane(0, 3)
     relay_side(0, 0)
     relay_plane(1, 1)
+    recurrence_inputs(1 - y, (0,), False)
     across(1, 1 - y).wait_recv()
     to_core(1 - y, 1, core, 3).start()
+    within_rows(1 - y, (0,))
+    relay_plane(1, 2)
     to_core(1 - y, 1, 1 - core, 3).wait_recv()
     attention_inputs((3,))
-    relay_plane(1, 2)
     relay_plane(1, 3)
     for k in range(1, 4):
         relay_side(0, k)
     relay_plane(2, 0)
-    recurrence_inputs(1 - y, False)
+    recurrence_inputs(1 - y, (1,), False)
     relay_side(1, 0)
     relay_side(1, 1)
     relay_plane(2, 1)
-    within_rows(1 - y, (0,))
+    within_rows(1 - y, (1,))
+    local_states()
+    send_pair()
+    relay_plane(2, 2)
+    relay_plane(2, 3)
     relay_side(1, 2)
     relay_side(1, 3)
-    relay_plane(2, 2)
-    within_rows(1 - y, (1,))
-    relay_plane(2, 3)
-    local_states()
-    send_pair()
     lam_copy.wait_recv()
     for phase in near:
         for origin in range(2):

time: 51.5 us -> 48.6 us (0.944)
  Pallas kernels: 49.5 us -> 46.5 us
    pallas_call x1, Pallas kernels: 49.5 us -> 46.5 us  [on_device(): pl.pallas_call(functools.partial(fused_kernel, ranks, tp, heads, planes),...]
where the time goes in v6:
time: 48.6 us; the launch traced here: 48.4 us
  Pallas kernels  46.5 us (96%)
  local copies, waits for them, and re-layouts  1.88 us (4%)
    pallas_call x1, Pallas kernels, on_device(): pl.pallas_call(functools.partial(fused_kernel, ranks, tp, heads, planes),...  46.5 us
    unnamed x1, local copies, waits for them, and re-layouts  1.88 us

profile of v6, /device:TPU:0, one launch (start us, length us, event | category | flops | bytes accessed | tf_op | source)
XLA Modules:
  0.0 48.4 jit_solution(4575969662272146627)
XLA Ops:
  0.0 46.5 %shard_map.163 = bf16[128,2048]{1,0:T(8,128)(2,1)} custom-call(bf16[128,2048]{1,0:T(8,128)(2,1)} %tokens_in.1, f32[1,2048]{1,0:T(1,128)} %bitcast.5, bf16[2048,256]{1,0:T(8,128)(2,1)} %w_key.1, bf16[2048,256]{1,0:T(8,128)(2,1)} %w_value.1, bf16[2048,256]{1,0:T(8,128)(2,1)} %w_query.1, bf16[2048,256]{1,0:T(8,128)(2,1)} %w_rq.1, bf16[2048,256]{1,0:T(8,128)(2,1)} %w_fwd.1, ...), custom_call_target="tpu_custom_call" | custom-call | flops 10000000000 | bytes 10000000 | tf_op jit(solution)/shard_map/pallas_call | solution.py:1186
  46.6 1.9 %copy.19 = bf16[128,2048]{1,0:T(8,128)(2,1)} copy(bf16[128,2048]{1,0:T(8,128)(2,1)} %shard_map.163) | data formatting | bytes 1048576

commit v7 on v6

--- a/solution.py
+++ b/solution.py
@@ -1052,7 +1052,7 @@
     units = tiles_of(every, near_keys)
     side_tile = 1 - lax.div(2 * z, planes)
     for tile in (side_tile, 1 - side_tile):
-        units += [(q_phase, tile, far_keys) for q_phase in every]
+        units += [(q_phase, tile, far_keys) for q_phase in far + near]
     before = {
         1: [call(relay_plane, 3, 0)],
         2: [call(relay_plane, 3, 1)] + all_of(relay_side, 2, range(1)),

time: 48.6 us -> 48.1 us (0.990)
  no operation moved by 1% of the time
where the time goes in v7:
time: 48.1 us; the launch traced here: 48 us
  Pallas kernels  46.1 us (96%)
  local copies, waits for them, and re-layouts  1.88 us (4%)
    pallas_call x1, Pallas kernels, on_device(): pl.pallas_call(functools.partial(fused_kernel, ranks, tp, heads, planes),...  46.1 us
    unnamed x1, local copies, waits for them, and re-layouts  1.88 us

profile of v7, /device:TPU:0, one launch (start us, length us, event | category | flops | bytes accessed | tf_op | source)
XLA Modules:
  0.0 48.0 jit_solution(14156500337502497896)
XLA Ops:
  0.0 46.1 %shard_map.163 = bf16[128,2048]{1,0:T(8,128)(2,1)} custom-call(bf16[128,2048]{1,0:T(8,128)(2,1)} %tokens_in.1, f32[1,2048]{1,0:T(1,128)} %bitcast.5, bf16[2048,256]{1,0:T(8,128)(2,1)} %w_key.1, bf16[2048,256]{1,0:T(8,128)(2,1)} %w_value.1, bf16[2048,256]{1,0:T(8,128)(2,1)} %w_query.1, bf16[2048,256]{1,0:T(8,128)(2,1)} %w_rq.1, bf16[2048,256]{1,0:T(8,128)(2,1)} %w_fwd.1, ...), custom_call_target="tpu_custom_call" | custom-call | flops 10000000000 | bytes 10000000 | tf_op jit(solution)/shard_map/pallas_call | solution.py:1186
  46.1 1.9 %copy.19 = bf16[128,2048]{1,0:T(8,128)(2,1)} copy(bf16[128,2048]{1,0:T(8,128)(2,1)} %shard_map.163) | data formatting | bytes 1048576
